TPU v7x, 256 devices: a 4x2x16 block of a 4x16x16 slice. The times are simulated.
256 devices in a mesh: grp: 2 (over y), sp: 32 (over z, core), tp: 4 (over x).
Axes of the slice: x: 4, y: 2, z: 16, core: 2. Of those that a mesh axis runs over, the one named last changes fastest.
The devices are a block of a 4x16x16 slice.
Arguments:
- carryover_vector: bfloat16 [16384, 2048], P(('grp', 'sp', 'tp')), parts along dimension 0, may hold values from -6 to 6
- channel_source_entries: bfloat16 [16384, 1024], P(('grp', 'sp'), 'tp'), parts along dimension 0, may hold values from -6 to 6
- final_modulation_vector: bfloat16 [16384, 1024], P(('grp', 'sp'), 'tp'), parts along dimension 0, may hold values from -54 to 54
- entering_basis_matrix: bfloat16 [16384, 512], P(('grp', 'sp'), 'tp'), parts along dimension 0, may hold values from -6 to 6
- readout_basis_matrix: bfloat16 [16384, 512], P(('grp', 'sp'), 'tp'), parts along dimension 0, may hold values from -6 to 6
- raw_stride_amount: float32 [16384, 16], P(('grp', 'sp'), 'tp'), parts along dimension 0, may hold values from -6 to 5
- extra_log_attenuation: float32 [16384, 16], P(('grp', 'sp'), 'tp'), parts along dimension 0, may hold values from -1.4 to 0
- channel_fading_rate: float32 [16], P('tp'), may hold values from 0 to 0.1, as said below
- channel_source_kernel: float32 [4, 1024], P(None, 'tp'), may hold values from -3 to 3
- entering_basis_kernel: float32 [4, 512], P(None, 'tp'), may hold values from -3 to 3
- readout_basis_kernel: float32 [4, 512], P(None, 'tp'), may hold values from -3 to 3
- modulated_rescaling_vector: float32 [1024], replicated, may hold values from 0.1 to 1.9
- blender_final_matrix: bfloat16 [1024, 2048], replicated, may hold values from -0.1875 to 0.1875
- specialist_rescaling_vector: float32 [2048], replicated, may hold values from 0.1 to 1.9
- specialist_gating_matrices: bfloat16 [64, 2048, 1024], P('sp', None, 'tp'), may hold values from -0.125 to 0.125
- widening_matrices: bfloat16 [64, 2048, 1024], P('sp', None, 'tp'), may hold values from -0.125 to 0.125
- contracting_matrices: bfloat16 [64, 1024, 2048], P('sp', 'tp'), may hold values from -0.1875 to 0.1875
- assigned_specialist_ids: int32 [16384, 2], P(('grp', 'sp')), parts along dimension 0, may hold values from 0 to 63, as said below
- specialist_choice_affinity: float32 [16384, 2], P(('grp', 'sp', 'tp')), parts along dimension 0, may hold values from -6 to 6
- cluster_chance: float32 [16384], P(('grp', 'sp', 'tp')), parts along dimension 0, may hold values from 0.25 to 1
Outputs:
- layer_out: bfloat16 [16384, 2048], P(('grp', 'sp', 'tp')), parts along dimension 0
There are 2 independent parts, one for each index of `grp`. A program takes and returns all parts, laid end to end along the dimension named above; an argument that names none is the same for every part. Nothing has to cross between parts.
Inputs may be any that keep to these rules, and one draw needn't show every extreme that they name: `assigned_specialist_ids`: each row names 2 different experts of one group: the experts g * 16 to (g + 1) * 16 - 1 for one g below 4. In each aligned block of 64 rows (the rows of one device) no expert is named by more than 4 rows, and every expert of one group, the same group in all blocks, is named by exactly 4 rows of every block. `channel_fading_rate`: positive.
All inputs are finite; a program needn't handle non-finite values.
Results may differ from a plain program's by a relative error of at most 0.015.
Values may be sent and summed in bfloat16 or wider, within the bound.
A program may use at most 64 MiB of HBM per device.

v0:
```python
import jax
import jax.numpy as jnp
from jax import lax
from jax.sharding import Mesh
from jax.sharding import PartitionSpec as P

HEAD_DIM = 64
STATE = 128
BLOCK = 64
SP = ("sp_0", "sp_1")
GRP_SP_TP = ("grp", "sp_0", "sp_1", "tp")
GRP_SP = ("grp", "sp_0", "sp_1")


EPS = 1e-06


def filled_with(x, identity):
    return jax.tree.map(
        lambda part, zero: jnp.zeros_like(part) + jnp.asarray(zero, part.dtype), x, identity
    )


def carried_in(x, axes, combine, identity):
    before = start = filled_with(x, identity)
    subtotal = x
    for axis in reversed(axes):
        size, index = (lax.axis_size(axis), lax.axis_index(axis))
        pieces = jax.tree.map(
            lambda part, kind: lax.all_gather(part.astype(kind), axis),
            subtotal,
            (jnp.bfloat16, jnp.bfloat16),
        )
        inside, subtotal = (start, start)
        for k in range(size):
            passed = k < index
            subtotal = combine(
                subtotal, jax.tree.map(lambda part, own: part[k].astype(own.dtype), pieces, x)
            )
            inside = jax.tree.map(lambda new, old: jnp.where(passed, new, old), subtotal, inside)
        before = combine(inside, before)
    return before


def from_behind(x, axis, by):
    size = lax.axis_size(axis)
    pairs = [(i, i + by) for i in range(size) if 0 <= i + by < size]
    return lax.ppermute(x, axis, pairs)


def for_sending(x):
    return jax.tree.map(lambda a: a.astype(jnp.bfloat16) if a.dtype == jnp.float32 else a, x)


def split_up(x, dim, size):
    shape = x.shape
    blocks = x.reshape(*shape[:dim], size, shape[dim] // size, *shape[dim + 1 :])
    return jnp.moveaxis(blocks, dim, 0)


def summed_on_arrival(x, axis, dim):
    size = lax.axis_size(axis)
    blocks = lax.all_to_all(split_up(x, dim, size), axis, 0, 0, tiled=True)
    return jnp.sum(blocks.astype(jnp.float32), axis=0)


def causal_conv(signal, earlier, weights):
    kernel_len = weights.shape[0]
    length = signal.shape[0]
    joined = jnp.concatenate([earlier, signal], axis=0).astype(jnp.float32)
    accumulated = jnp.zeros((length, signal.shape[1]), jnp.float32)
    for offset in range(kernel_len):
        accumulated = accumulated + weights[offset][None, :] * joined[offset : offset + length]
    return jax.nn.silu(accumulated)


def link_states(earlier, later):
    return (earlier[0] * later[0], earlier[1] * later[0][..., None, None] + later[1])


def device_states(scaled_in, log_attenuation, keys_b, queries_c, groups_here):
    length = scaled_in.shape[0]
    blocks = length // BLOCK
    per_group = scaled_in.shape[1] // groups_here
    scaled_in = scaled_in.reshape(blocks, BLOCK, groups_here, per_group, HEAD_DIM)
    log_attenuation = log_attenuation.reshape(blocks, BLOCK, groups_here, per_group)
    keys_b = keys_b.reshape(blocks, BLOCK, groups_here, STATE)
    queries_c = queries_c.reshape(blocks, BLOCK, groups_here, STATE)
    running = jnp.cumsum(log_attenuation, axis=1)
    lower_mask = jnp.tril(jnp.ones((BLOCK, BLOCK), dtype=bool))
    between = running[:, :, None] - running[:, None, :]
    decays = jnp.exp(jnp.where(lower_mask[None, :, :, None, None], between, -jnp.inf))
    scores = jnp.einsum("blgn,bsgn->blsg", queries_c, keys_b)
    inside = jnp.einsum("blsg,blsgr,bsgrp->blgrp", scores, decays, scaled_in)
    totals = running[:, -1]
    remain = jnp.exp(totals[:, None] - running)
    block_states = jnp.einsum("bsgn,bsgr,bsgrp->bgrpn", keys_b, remain, scaled_in)

    def advance(carried, pieces):
        return (carried * jnp.exp(pieces[1])[..., None, None] + pieces[0], carried)

    initial = jnp.zeros(block_states.shape[1:], jnp.float32)
    own_state, entering = lax.scan(advance, initial, (block_states, totals))
    own_decay = jnp.exp(jnp.sum(totals, axis=0))
    _, incoming = carried_in(
        (own_decay, own_state),
        SP,
        link_states,
        (jnp.ones_like(own_decay), jnp.zeros_like(own_state)),
    )
    preceding = jnp.exp(jnp.cumsum(totals, axis=0) - totals)
    entering = entering + preceding[..., None, None] * incoming[None]
    outside = jnp.einsum("blgn,bgrpn,blgr->blgrp", queries_c, entering, jnp.exp(running))
    return (inside + outside).reshape(length, -1)


def fetch_rows(tokens, sources):
    present = sources >= 0
    picked = jnp.take(tokens, jnp.maximum(sources, 0), axis=0)
    return jnp.where(present[:, None], picked, jnp.zeros_like(picked))


def slot_tables(chosen_ids, quarters, row_count, experts, capacity):
    picks = chosen_ids.shape[1]
    flat_ids = chosen_ids.reshape(quarters, row_count * picks)
    member = (flat_ids[..., None] == jnp.arange(experts, dtype=jnp.int32)).astype(jnp.int32)
    position = jnp.sum((jnp.cumsum(member, axis=1) - member) * member, axis=2)
    quarter_ids = jnp.arange(quarters, dtype=jnp.int32)[:, None]
    slot_index = flat_ids * (quarters * capacity) + quarter_ids * capacity + position
    token_index = (
        quarter_ids * row_count + jnp.arange(row_count * picks, dtype=jnp.int32)[None, :] // picks
    )
    sources = (
        jnp.full((experts * quarters * capacity,), -1, jnp.int32)
        .at[slot_index.reshape(-1)]
        .set(token_index.reshape(-1))
    )
    return (sources, position)


def per_device(
    carryover_vector,
    channel_source_entries,
    final_modulation_vector,
    entering_basis_matrix,
    readout_basis_matrix,
    raw_stride_amount,
    extra_log_attenuation,
    channel_fading_rate,
    channel_source_kernel,
    entering_basis_kernel,
    readout_basis_kernel,
    modulated_rescaling_vector,
    blender_final_matrix,
    specialist_rescaling_vector,
    specialist_gating_matrices,
    widening_matrices,
    contracting_matrices,
    assigned_specialist_ids,
    specialist_choice_affinity,
    cluster_chance,
):
    length = channel_source_entries.shape[0]
    row_count = carryover_vector.shape[0]
    model_width = carryover_vector.shape[1]
    heads_here = channel_fading_rate.shape[0]
    groups_here = entering_basis_matrix.shape[1] // STATE
    tp_index = lax.axis_index("tp")
    rim_rows = channel_source_kernel.shape[0] - 1
    neighbours = from_behind(
        (
            channel_source_entries[length - rim_rows :],
            entering_basis_matrix[length - rim_rows :],
            readout_basis_matrix[length - rim_rows :],
        ),
        SP,
        1,
    )
    inputs_x = causal_conv(channel_source_entries, neighbours[0], channel_source_kernel)
    keys_b = causal_conv(entering_basis_matrix, neighbours[1], entering_basis_kernel)
    queries_c = causal_conv(readout_basis_matrix, neighbours[2], readout_basis_kernel)
    channel_stride_amount = jax.nn.softplus(raw_stride_amount)
    log_attenuation = extra_log_attenuation - channel_fading_rate[None, :] * channel_stride_amount
    heads_x = inputs_x.reshape(length, heads_here, HEAD_DIM)
    mixed = device_states(
        heads_x * channel_stride_amount[:, :, None], log_attenuation, keys_b, queries_c, groups_here
    )
    gated = mixed * jax.nn.silu(final_modulation_vector.astype(jnp.float32))
    own_rows = lax.all_to_all(
        for_sending(gated), "tp", split_axis=0, concat_axis=1, tiled=True
    ).astype(gated.dtype)
    normed = (
        own_rows
        * lax.rsqrt(jnp.mean(own_rows * own_rows, axis=1, keepdims=True) + EPS)
        * modulated_rescaling_vector[None, :]
    ).astype(jnp.bfloat16)
    middle = (
        carryover_vector.astype(jnp.float32)
        + jnp.dot(normed, blender_final_matrix, preferred_element_type=jnp.float32)
    ).astype(jnp.bfloat16)
    middle_wide = middle.astype(jnp.float32)
    expert_input = (
        middle_wide
        * lax.rsqrt(jnp.mean(middle_wide * middle_wide, axis=1, keepdims=True) + EPS)
        * specialist_rescaling_vector[None, :]
    ).astype(jnp.bfloat16)
    sp_count = lax.axis_size(SP)
    local_experts = specialist_gating_matrices.shape[0]
    experts = sp_count * local_experts
    picks = assigned_specialist_ids.shape[1]
    capacity = 2 * row_count * picks // experts
    own_ids = lax.dynamic_slice_in_dim(assigned_specialist_ids, tp_index * row_count, row_count, 0)
    sources, position = slot_tables(own_ids, 1, row_count, experts, capacity)
    own_position = position[0]
    outgoing = fetch_rows(expert_input, sources).reshape(
        sp_count, local_experts, 1, capacity, model_width
    )
    received = lax.all_to_all(outgoing, SP, split_axis=0, concat_axis=0, tiled=True)
    arrived = lax.all_gather(received, "tp", axis=2, tiled=True)
    gate_value = jnp.einsum(
        "slqcd,ldf->slqcf", arrived, specialist_gating_matrices, preferred_element_type=jnp.float32
    )
    up_value = jnp.einsum(
        "slqcd,ldf->slqcf", arrived, widening_matrices, preferred_element_type=jnp.float32
    )
    hidden = (jax.nn.silu(gate_value) * up_value).astype(jnp.bfloat16)
    partial_value = jnp.einsum(
        "slqcf,lfd->slqcd", hidden, contracting_matrices, preferred_element_type=jnp.float32
    )
    width_total = summed_on_arrival(partial_value.astype(jnp.bfloat16), "tp", 2).astype(
        jnp.bfloat16
    )
    returned = lax.all_to_all(width_total, SP, split_axis=0, concat_axis=0, tiled=True)
    answers = returned.reshape(experts * capacity, model_width)
    own_slots = own_ids.reshape(-1) * capacity + own_position
    gathered = (
        jnp.take(answers, own_slots, axis=0)
        .reshape(row_count, picks, model_width)
        .astype(jnp.float32)
    )
    lifted = jnp.exp(specialist_choice_affinity)
    shares = cluster_chance[:, None] * lifted / jnp.sum(lifted, axis=1, keepdims=True)
    return (middle_wide + jnp.sum(shares[:, :, None] * gathered, axis=1)).astype(jnp.bfloat16)


def solution(mesh):
    finer = Mesh(
        mesh.devices.reshape(mesh.shape["grp"], 16, 2, mesh.shape["tp"]),
        ("grp", "sp_0", "sp_1", "tp"),
    )
    return jax.shard_map(
        per_device,
        mesh=finer,
        in_specs=(
            P(GRP_SP_TP, None),
            P(GRP_SP, "tp"),
            P(GRP_SP, "tp"),
            P(GRP_SP, "tp"),
            P(GRP_SP, "tp"),
            P(GRP_SP, "tp"),
            P(GRP_SP, "tp"),
            P("tp"),
            P(None, "tp"),
            P(None, "tp"),
            P(None, "tp"),
            P(),
            P(),
            P(),
            P(SP, None, "tp"),
            P(SP, None, "tp"),
            P(SP, "tp", None),
            P(GRP_SP, None),
            P(GRP_SP_TP, None),
            P(GRP_SP_TP),
        ),
        out_specs=P(GRP_SP_TP, None),
        check_vma=False,
    )
```

profile of v0, /device:TPU:33, one launch (start us, length us, event | category | flops | bytes accessed | tf_op | source)
XLA Modules:
  0.0 418.4 jit_solution(9210774802349872012)
XLA Ops:
  7.4 5.7 %collective-permute-start.2 = (bf16[3,256]{1,0:T(4,128)(2,1)S(1)}, bf16[3,256]{1,0:T(4,128)(2,1)S(1)}, u32[]{:S(2)}, u32[]{:S(2)}) collective-permute-start(bf16[3,256]{1,0:T(4,128)(2,1)S(1)} %slice.211), channel_id=1, source_target_pairs={{0,4},{4,8},{8,12},{12,16},{16,20},{20,24},{24,28},{28,32},{32,36}... | collective-permute-start | bytes 4616 | tf_op jit(solution)/shard_map/ppermute | solution.py:48
  13.8 1.9 collective-permute-start
  17.1 4.8 %collective-permute-start.1 = (bf16[3,128]{1,0:T(4,128)(2,1)}, bf16[3,128]{1,0:T(4,128)(2,1)}, u32[]{:S(2)}, u32[]{:S(2)}) collective-permute-start(bf16[3,128]{1,0:T(4,128)(2,1)} %slice.202), channel_id=1, source_target_pairs={{0,4},{4,8},{8,12},{12,16},{16,20},{20,24},{24,28},{28,32},{32,36}... | collective-permute-start | bytes 2312 | tf_op jit(solution)/shard_map/ppermute | solution.py:48
  27.3 14.5 %all-reduce = bf16[8]{0:T(256)(128)(2,1)S(1)} all-reduce(bf16[8]{0:T(256)(128)(2,1)S(1)} %dynamic-update-slice), channel_id=2, replica_groups=mesh['grp'=2,'sp_0'=16,'sp_1'=2,'tp'=4] {'sp_1'}, use_global_device_ids=true, to_apply=%add | all-reduce | flops 8 | bytes 32
  49.6 5.7 %while.13 = (s32[]{:T(128)}, f32[1,4,64,128]{3,2,1,0:T(8,128)S(1)}, f32[4,1,4,64,128]{4,3,2,1,0:T(8,128)}, f32[4,1,4]{2,1,0:T(1,128)}, f32[4,1,4,64,128]{4,3,2,1,0:T(8,128)S(1)}, /*index=5*/s32[]{:T(128)}, s32[]{:T(128)}) while((s32[]{:T(128)}, f32[1,4,64,128]{3,2,1,0:T(8,128)S(1)}, f32[4,1,4,64,128]{4,3,2,1,0:T(8,128)}, ...), condition=%wide.region_2.3_spmd.clone, body=%wide.region_1.2_spmd.clone.sunk | while | flops 131075 | bytes 656016 | solution.py:103
  55.3 2.0 all-gather.1
  57.2 1.4 fusion.68
  60.6 25.0 %all_gather.22 = bf16[16,1,4]{2,1,0:T(2,128)(2,1)S(1)} all-gather(bf16[1,1,4]{2,1,0:T(2,128)(2,1)} %get-tuple-element.121), channel_id=1, replica_groups=mesh['grp'=2,'sp_0'=16,'sp_1'=2,'tp'=4] {'sp_0'}, dimensions={0}, use_global_device_ids=true | all-gather | bytes 136 | tf_op jit(solution)/shard_map/all_gather | solution.py:30
  91.8 24.7 %all-gather.5.cloned.1.call-done = bf16[16,1,4,64,128]{4,3,2,1,0:T(8,128)(2,1)} async-done(((bf16[1,1,4,64,128]{4,3,2,1,0:T(8,128)(2,1)}), bf16[16,1,4,64,128]{4,3,2,1,0:T(8,128)(2,1)}) %all-gather.5.cloned.1.call-update) | async-done | bytes 1048592 | tf_op jit(solution)/shard_map/all_gather | solution.py:30
  116.5 1.7 fusion.65
  118.2 1.5 fusion.21
  121.4 1.6 fusion.53
  123.0 4.0 all-to-all-start
  127.0 4.8 %all-to-all-done = bf16[4,64,256]{2,1,0:T(8,128)(2,1)S(1)} async-done(((bf16[4,64,256]{2,1,0:T(8,128)(2,1)}), bf16[4,64,256]{2,1,0:T(8,128)(2,1)S(1)}, u32[]{:S(2)}, u32[]{:S(2)}) %all-to-all-start) | async-done | bytes 131104 | tf_op jit(solution)/shard_map/all_to_all | solution.py:189
  132.1 3.2 multiply_reduce_fusion.1
  136.3 1.4 gather_fusion
  138.8 1.9 select_bitcast_fusion
  140.8 76.2 %all_to_all.28 = bf16[32,2,1,4,2048]{4,3,2,1,0:T(4,128)(2,1)S(1)} all-to-all(bf16[32,2,1,4,2048]{4,3,2,1,0:T(4,128)(2,1)S(1)} %select_bitcast_fusion), channel_id=1, replica_groups=mesh['grp'=2,'sp_0'=16,'sp_1'=2,'tp'=4] {'sp_0','sp_1'}, dimensions={0} | all-to-all | bytes 2097152 | tf_op jit(solution)/shard_map/all_to_all | solution.py:218
  217.0 1.6 copy.91
  218.6 44.0 %all-gather.7.cloned.1.call-done = bf16[32,2,4,4,2048]{4,0,3,2,1:T(8,128)(2,1)} async-done(((bf16[32,2,1,4,2048]{4,0,3,2,1:T(8,128)(2,1)}), bf16[32,2,4,4,2048]{4,0,3,2,1:T(8,128)(2,1)}) %all-gather.7.cloned.1.call-update) | async-done | bytes 4194320 | tf_op jit(solution)/shard_map/all_gather | solution.py:219
  262.6 4.1 fusion.9
  266.7 7.3 %convert_bitcast_fusion = bf16[4,32,2,1,4,2048]{5,1,4,0,2,3:T(8,128)(2,1)} fusion(bf16[2,256,2048]{2,1,0:T(8,128)(2,1)S(1)} %copy-done, bf16[32,2,4,4,2048]{4,0,3,2,1:T(8,128)(2,1)} %all-gather.7.cloned.1.call-done, bf16[2,2048,256]{2,1,0:T(8,128)(2,1)} %param.37, f32[32,2,4,4,256]{4,0,3,2,1:T(8,128)S(1)} %fusion.9), kind=kOutput, calls=%fused_computation.8 | convolution fusion | flops 2151153664 | bytes 13631488 | tf_op jit(solution)/shard_map/slqcf,lfd->slqcd/dot_general | solution.py:227
  274.0 2.5 copy.92
  276.5 51.3 %all_to_all.29 = bf16[4,32,2,1,4,2048]{5,1,4,2,3,0:T(8,128)(2,1)} all-to-all(bf16[4,32,2,1,4,2048]{5,1,4,2,3,0:T(8,128)(2,1)S(1)} %copy.92), channel_id=1, replica_groups=mesh['grp'=2,'sp_0'=16,'sp_1'=2,'tp'=4] {'tp'}, dimensions={0} | all-to-all | bytes 8388608 | tf_op jit(solution)/shard_map/all_to_all | solution.py:63
  327.8 3.1 reduce_sum.79
  330.9 1.9 copy.94
  332.8 14.3 %all-to-all-start.3 = ((bf16[32,2,1,4,2048]{4,3,1,2,0:T(4,128)(2,1)}), bf16[32,2,1,4,2048]{4,3,1,2,0:T(4,128)(2,1)}, u32[]{:S(2)}, u32[]{:S(2)}) async-start(bf16[32,2,1,4,2048]{4,3,1,2,0:T(4,128)(2,1)} %copy.94), calls=%async_computation.3 | async-start | bytes 2097152 | tf_op jit(solution)/shard_map/all_to_all | solution.py:233
  347.7 55.1 %all-to-all-done.3 = bf16[32,2,1,4,2048]{4,3,1,2,0:T(4,128)(2,1)} async-done(((bf16[32,2,1,4,2048]{4,3,1,2,0:T(4,128)(2,1)}), bf16[32,2,1,4,2048]{4,3,1,2,0:T(4,128)(2,1)}, u32[]{:S(2)}, u32[]{:S(2)}) %all-to-all-start.3) | async-done | bytes 1048608 | tf_op jit(solution)/shard_map/all_to_all | solution.py:233
  404.1 1.7 gather_fusion.1
  405.8 1.4 gather.15
  407.2 2.5 multiply_reduce_fusion
  409.7 1.8 add_convert_fusion
  (127 shorter events, 34.9 us)
Async XLA Ops:
  6.5 260.2 %copy-start = (bf16[2,256,2048]{2,1,0:T(8,128)(2,1)S(1)}, bf16[2,256,2048]{2,1,0:T(8,128)(2,1)}, u32[]{:S(2)}) copy-start(bf16[2,256,2048]{2,1,0:T(8,128)(2,1)} %param.38) | copy-start | bytes 6291460
  6.6 109.9 %all-gather.5.cloned.1.call-start = ((), (), s32[]{:S(2)}) async-start(), calls=%async_computation.4 | async-start | bytes 1114112 | tf_op jit(solution)/shard_map/all_gather | solution.py:30
  7.4 40.4 %collective-permute-start.2 = (bf16[3,256]{1,0:T(4,128)(2,1)S(1)}, bf16[3,256]{1,0:T(4,128)(2,1)S(1)}, u32[]{:S(2)}, u32[]{:S(2)}) collective-permute-start(bf16[3,256]{1,0:T(4,128)(2,1)S(1)} %slice.211), channel_id=1, source_target_pairs={{0,4},{4,8},{8,12},{12,16},{16,20},{20,24},{24,28},{28,32},{32,36}... | collective-permute-start | bytes 4616 | tf_op jit(solution)/shard_map/ppermute | solution.py:48
  13.8 33.0 %collective-permute-start = (bf16[3,128]{1,0:T(4,128)(2,1)S(1)}, bf16[3,128]{1,0:T(4,128)(2,1)S(1)}, u32[]{:S(2)}, u32[]{:S(2)}) collective-permute-start(bf16[3,128]{1,0:T(4,128)(2,1)S(1)} %slice.193), channel_id=1, source_target_pairs={{0,4},{4,8},{8,12},{12,16},{16,20},{20,24},{24,28},{28,32},{32,36}... | collective-permute-start | bytes 2312 | tf_op jit(solution)/shard_map/ppermute | solution.py:48
  17.1 73.7 %collective-permute-start.1 = (bf16[3,128]{1,0:T(4,128)(2,1)}, bf16[3,128]{1,0:T(4,128)(2,1)}, u32[]{:S(2)}, u32[]{:S(2)}) collective-permute-start(bf16[3,128]{1,0:T(4,128)(2,1)} %slice.202), channel_id=1, source_target_pairs={{0,4},{4,8},{8,12},{12,16},{16,20},{20,24},{24,28},{28,32},{32,36}... | collective-permute-start | bytes 2312 | tf_op jit(solution)/shard_map/ppermute | solution.py:48
  24.3 24.4 %copy-start.6 = (f32[4,1,1,4]{3,2,1,0:T(1,128)}, f32[4,1,1,4]{3,2,1,0:T(1,128)S(1)}, u32[]{:S(2)}) copy-start(f32[4,1,1,4]{3,2,1,0:T(1,128)S(1)} %get-tuple-element.89) | copy-start | bytes 196
  43.2 3.5 copy-start.7
  43.9 4.9 %copy-start.11 = (s32[128]{0:T(128)}, s32[128]{0:T(128)S(1)}, u32[]{:S(2)}) copy-start(s32[128]{0:T(128)S(1)} %select_reduce_fusion) | copy-start | bytes 1540
  48.8 42.0 %copy-start.3 = (bf16[256,128]{1,0:T(8,128)(2,1)S(1)}, bf16[256,128]{1,0:T(8,128)(2,1)}, u32[]{:S(2)}) copy-start(bf16[256,128]{1,0:T(8,128)(2,1)} %param.26) | copy-start | bytes 196612
  91.7 40.4 %copy-start.2 = (bf16[64,2048]{1,0:T(8,128)(2,1)S(1)}, bf16[64,2048]{1,0:T(8,128)(2,1)}, u32[]{:S(2)}) copy-start(bf16[64,2048]{1,0:T(8,128)(2,1)} %param.22) | copy-start | bytes 786436
  91.7 40.4 %copy-start.10 = (f32[1024]{0:T(1024)S(1)}, f32[1024]{0:T(1024)}, u32[]{:S(2)}) copy-start(f32[1024]{0:T(1024)} %param.33) | copy-start | bytes 12292
  121.0 15.1 %copy-start.9 = (f32[2048]{0:T(1024)S(1)}, f32[2048]{0:T(1024)}, u32[]{:S(2)}) copy-start(f32[2048]{0:T(1024)} %param.35) | copy-start | bytes 24580
  123.0 8.8 %all-to-all-start = ((bf16[4,64,256]{2,1,0:T(8,128)(2,1)}), bf16[4,64,256]{2,1,0:T(8,128)(2,1)S(1)}, u32[]{:S(2)}, u32[]{:S(2)}) async-start(bf16[4,64,256]{2,1,0:T(8,128)(2,1)} %bitcast.53), calls=%async_computation | async-start | bytes 262144 | tf_op jit(solution)/shard_map/all_to_all | solution.py:189
  127.0 135.6 %all-gather.7.cloned.1.call-start = ((), (), s32[]{:S(2)}) async-start(), calls=%async_computation.5 | async-start | bytes 5242880 | tf_op jit(solution)/shard_map/all_gather | solution.py:219
  135.3 0.8 copy-start.1
  136.2 2.6 copy-start.4
  136.2 2.6 copy-start.5
  327.8 19.3 %copy-start.12 = (s32[128]{0:T(128)S(1)}, s32[128]{0:T(128)}, u32[]{:S(2)}) copy-start(s32[128]{0:T(128)} %copy-done.11) | copy-start | bytes 1540
  327.8 19.5 %copy-start.8 = (s32[64,2]{0,1:T(2,128)S(1)}, s32[64,2]{0,1:T(2,128)}, u32[]{:S(2)}) copy-start(s32[64,2]{0,1:T(2,128)} %copy-done.7) | copy-start | bytes 1540
  327.8 19.7 %copy-start.13 = (f32[64,2]{0,1:T(2,128)S(1)}, f32[64,2]{0,1:T(2,128)}, u32[]{:S(2)}) copy-start(f32[64,2]{0,1:T(2,128)} %param.40) | copy-start | bytes 1540
  327.8 19.7 %copy-start.15 = (f32[64]{0:T(128)S(1)}, f32[64]{0:T(128)}, u32[]{:S(2)}) copy-start(f32[64]{0:T(128)} %param.41) | copy-start | bytes 772
  327.8 19.8 %copy-start.14 = (s32[128]{0:T(128)S(1)}, s32[128]{0:T(128)}, u32[]{:S(2)}) copy-start(s32[128]{0:T(128)} %fusion.70) | copy-start | bytes 1540
  332.8 69.9 %all-to-all-start.3 = ((bf16[32,2,1,4,2048]{4,3,1,2,0:T(4,128)(2,1)}), bf16[32,2,1,4,2048]{4,3,1,2,0:T(4,128)(2,1)}, u32[]{:S(2)}, u32[]{:S(2)}) async-start(bf16[32,2,1,4,2048]{4,3,1,2,0:T(4,128)(2,1)} %copy.94), calls=%async_computation.3 | async-start | bytes 2097152 | tf_op jit(solution)/shard_map/all_to_all | solution.py:233
Sparse Core Ops, SparseCore 0:
  58.8 57.6 all-gather.4
  218.7 43.8 all-gather.6
where the time goes:
time: 420 us; the launch traced here: 418 us
  blocking collectives  169 us (40%)
  waiting for transfers between devices  129 us (31%)
  starting transfers between devices  30.8 us (7%)
  local copies, waits for them, and re-layouts  29.3 us (7%)
  other arithmetic  28.5 us (7%)
  matrix products  17.5 us (4%)
  between operations  14.6 us (3%)
    all_to_all x1, blocking collectives, per_device(): lax.all_to_all(outgoing, SP, split_axis=0, concat_axis=0, tiled=True)  76.2 us
    all_to_all x1, waiting for transfers between devices, per_device(): lax.all_to_all(width_total, SP, split_axis=0, concat_axis=0, tiled=True)  55.1 us
    all_to_all x1, blocking collectives, summed_on_arrival(): blocks = lax.all_to_all(split_up(x, dim, size), axis, 0, 0, tiled=True)  51.3 us
    all_gather x1, waiting for transfers between devices, per_device(): arrived = lax.all_gather(received, 'tp', axis=2, tiled=True)  44 us
    all_gather x2, blocking collectives, carried_in(): lax.all_gather(part.astype(kind), axis)  26.9 us
    all_gather x1, waiting for transfers between devices, carried_in(): lax.all_gather(part.astype(kind), axis)  24.7 us
    unnamed x1, blocking collectives  14.5 us
    all_to_all x1, starting transfers between devices, per_device(): lax.all_to_all(width_total, SP, split_axis=0, concat_axis=0, tiled=True)  14.3 us
  transfers between devices with their start and end apart: 7, of which 4 were waited for; matrix products, arithmetic and copies ran while one was open for 7% of the time, Pallas kernels for 0%

commit v1 on v0

--- a/solution.py
+++ b/solution.py
@@ -1,6 +1,10 @@
+import functools
+
 import jax
 import jax.numpy as jnp
 from jax import lax
+from jax.experimental import pallas as pl
+from jax.experimental.pallas import tpu as pltpu
 from jax.sharding import Mesh
 from jax.sharding import PartitionSpec as P
 
@@ -114,28 +118,240 @@
     return (inside + outside).reshape(length, -1)
 
 
-def fetch_rows(tokens, sources):
-    present = sources >= 0
-    picked = jnp.take(tokens, jnp.maximum(sources, 0), axis=0)
-    return jnp.where(present[:, None], picked, jnp.zeros_like(picked))
-
-
-def slot_tables(chosen_ids, quarters, row_count, experts, capacity):
-    picks = chosen_ids.shape[1]
-    flat_ids = chosen_ids.reshape(quarters, row_count * picks)
-    member = (flat_ids[..., None] == jnp.arange(experts, dtype=jnp.int32)).astype(jnp.int32)
-    position = jnp.sum((jnp.cumsum(member, axis=1) - member) * member, axis=2)
-    quarter_ids = jnp.arange(quarters, dtype=jnp.int32)[:, None]
-    slot_index = flat_ids * (quarters * capacity) + quarter_ids * capacity + position
-    token_index = (
-        quarter_ids * row_count + jnp.arange(row_count * picks, dtype=jnp.int32)[None, :] // picks
-    )
-    sources = (
-        jnp.full((experts * quarters * capacity,), -1, jnp.int32)
-        .at[slot_index.reshape(-1)]
-        .set(token_index.reshape(-1))
-    )
-    return (sources, position)
+def hop(step):
+    half = (step + 1) // 2
+    return jnp.where(step % 2 == 1, half, -half)
+
+
+def greet(nz, nx):
+    z, x = lax.axis_index("sp_0"), lax.axis_index("tp")
+    barrier = pltpu.get_barrier_semaphore()
+
+    def signal(k, carry):
+        pl.semaphore_signal(barrier, inc=1, device_id={"sp_0": lax.rem(z + k, nz)})
+        return carry
+
+    lax.fori_loop(1, nz, signal, 0)
+    pl.semaphore_signal(barrier, inc=1, device_id={"tp": lax.rem(x + 1, nx)})
+    pl.semaphore_signal(barrier, inc=1, device_id={"tp": lax.rem(x + nx - 1, nx)})
+    pl.semaphore_wait(barrier, nz + 1)
+
+
+def dispatch_kernel(nz, nx, src, dst, zs, zr, xs, xr, fs, fr, here):
+    z, x = lax.axis_index("sp_0"), lax.axis_index("tp")
+    xp, xm = lax.rem(x + 1, nx), lax.rem(x + nx - 1, nx)
+    x2 = lax.rem(x + 2, nx)
+    greet(nz, nx)
+
+    def along_z(i):
+        to = lax.rem(z + hop(i) + nz, nz)
+        return pltpu.make_async_remote_copy(
+            src.at[:, to], dst.at[:, x, z], zs.at[i], zr.at[i], device_id={"sp_0": to}
+        )
+
+    def origin(i):
+        return lax.rem(z - hop(i) + nz, nz)
+
+    def along_x(i, way):
+        chunk = dst.at[:, x, origin(i)]
+        to = xp if way == 0 else xm
+        return pltpu.make_async_remote_copy(
+            chunk, chunk, xs.at[way, i], xr.at[way, i], device_id={"tp": to}
+        )
+
+    def further(i):
+        way = i % 2
+        chunk = dst.at[:, jnp.where(way == 0, xm, xp), origin(i)]
+        to = jnp.where(way == 0, xp, xm)
+        return pltpu.make_async_remote_copy(
+            chunk, chunk, fs.at[i], fr.at[i], device_id={"tp": to}
+        )
+
+    def arrived_x(i, way):
+        chunk = dst.at[:, jnp.where(way == 0, xm, xp), origin(i)]
+        return pltpu.make_async_remote_copy(
+            chunk, chunk, xs.at[way, i], xr.at[way, i], device_id={"tp": xp}
+        )
+
+    def arrived_far(i):
+        chunk = dst.at[:, x2, origin(i)]
+        return pltpu.make_async_remote_copy(
+            chunk, chunk, fs.at[i], fr.at[i], device_id={"tp": xp}
+        )
+
+    def send_z(i, carry):
+        along_z(i).start()
+        return carry
+
+    lax.fori_loop(1, nz, send_z, 0)
+    own = pltpu.make_async_copy(src.at[:, z], dst.at[:, x, z], here)
+    own.start()
+    own.wait()
+    along_x(0, 0).start()
+    along_x(0, 1).start()
+
+    def spread(i, carry):
+        pltpu.make_async_remote_copy(
+            src.at[:, z], dst.at[:, x, origin(i)], zs.at[i], zr.at[i], device_id={"tp": xp}
+        ).wait_recv()
+        along_x(i, 0).start()
+        along_x(i, 1).start()
+        arrived_x(i - 1, (i - 1) % 2).wait_recv()
+        further(i - 1).start()
+        return carry
+
+    lax.fori_loop(1, nz, spread, 0)
+    arrived_x(nz - 1, (nz - 1) % 2).wait_recv()
+    further(nz - 1).start()
+
+    def finish(i, carry):
+        arrived_x(i, (i + 1) % 2).wait_recv()
+        arrived_far(i).wait_recv()
+        along_x(i, 0).wait_send()
+        along_x(i, 1).wait_send()
+        further(i).wait_send()
+        return carry
+
+    lax.fori_loop(0, nz, finish, 0)
+
+    def sent(i, carry):
+        along_z(i).wait_send()
+        return carry
+
+    lax.fori_loop(1, nz, sent, 0)
+
+
+def dispatch(outgoing, nz, nx):
+    experts, _, rows, width = outgoing.shape
+    return pl.pallas_call(
+        functools.partial(dispatch_kernel, nz, nx),
+        out_shape=jax.ShapeDtypeStruct((experts, nx, nz, rows, width), outgoing.dtype),
+        in_specs=[pl.BlockSpec(memory_space=pltpu.VMEM)],
+        out_specs=pl.BlockSpec(memory_space=pltpu.VMEM),
+        scratch_shapes=[
+            pltpu.SemaphoreType.DMA((nz,)),
+            pltpu.SemaphoreType.DMA((nz,)),
+            pltpu.SemaphoreType.DMA((2, nz)),
+            pltpu.SemaphoreType.DMA((2, nz)),
+            pltpu.SemaphoreType.DMA((nz,)),
+            pltpu.SemaphoreType.DMA((nz,)),
+            pltpu.SemaphoreType.DMA,
+        ],
+        compiler_params=pltpu.CompilerParams(collective_id=1, has_side_effects=True),
+        name="dispatch",
+    )(outgoing)
+
+
+def collect_kernel(nz, nx, part, out, far, near, both, mine, total, fs, fr, ns, nr, bs, br, zs, zr, here):
+    z, x = lax.axis_index("sp_0"), lax.axis_index("tp")
+    xp, xm = lax.rem(x + 1, nx), lax.rem(x + nx - 1, nx)
+    x2 = lax.rem(x + 2, nx)
+    greet(nz, nx)
+
+    def step_of(s):
+        return nz - 1 - s
+
+    def goal(i):
+        return lax.rem(z + hop(i) + nz, nz)
+
+    def ahead(i):
+        return jnp.where(i % 2 == 0, xp, xm)
+
+    def behind(i):
+        return jnp.where(i % 2 == 0, xm, xp)
+
+    def send_far(i):
+        return pltpu.make_async_remote_copy(
+            part.at[:, x2, goal(i)], far.at[i], fs.at[i], fr.at[i], device_id={"tp": ahead(i)}
+        )
+
+    def send_near(i):
+        return pltpu.make_async_remote_copy(
+            part.at[:, behind(i), goal(i)], near.at[i], ns.at[i], nr.at[i], device_id={"tp": behind(i)}
+        )
+
+    def send_both(i):
+        return pltpu.make_async_remote_copy(
+            mine.at[i], both.at[i], bs.at[i], br.at[i], device_id={"tp": ahead(i)}
+        )
+
+    def send_z(i):
+        return pltpu.make_async_remote_copy(
+            total.at[i], out.at[:, z], zs.at[i], zr.at[i], device_id={"sp_0": goal(i)}
+        )
+
+    def first(i):
+        send_far(i).start()
+        send_near(i).start()
+
+    def second(i):
+        send_far(i).wait_recv()
+        mine[i] = (
+            part[:, ahead(i), goal(i)].astype(jnp.float32) + far[i].astype(jnp.float32)
+        ).astype(mine.dtype)
+        send_both(i).start()
+
+    def third(i):
+        send_near(i).wait_recv()
+        send_both(i).wait_recv()
+        total[i] = (
+            part[:, x, goal(i)].astype(jnp.float32)
+            + near[i].astype(jnp.float32)
+            + both[i].astype(jnp.float32)
+        ).astype(total.dtype)
+
+    first(step_of(0))
+    first(step_of(1))
+    second(step_of(0))
+
+    def turn(s, carry):
+        first(step_of(s))
+        second(step_of(s - 1))
+        third(step_of(s - 2))
+        send_z(step_of(s - 2)).start()
+        return carry
+
+    lax.fori_loop(2, nz, turn, 0)
+    second(step_of(nz - 1))
+    third(step_of(nz - 2))
+    send_z(step_of(nz - 2)).start()
+    third(step_of(nz - 1))
+    own = pltpu.make_async_copy(total.at[0], out.at[:, z], here)
+    own.start()
+    own.wait()
+
+    def finish(i, carry):
+        send_far(i).wait_send()
+        send_near(i).wait_send()
+        send_both(i).wait_send()
+        return carry
+
+    lax.fori_loop(0, nz, finish, 0)
+
+    def sent(i, carry):
+        send_z(i).wait_send()
+        pltpu.make_async_remote_copy(
+            total.at[i], out.at[:, lax.rem(z - hop(i) + nz, nz)], zs.at[i], zr.at[i], device_id={"tp": xp}
+        ).wait_recv()
+        return carry
+
+    lax.fori_loop(1, nz, sent, 0)
+
+
+def collect(part, nz, nx):
+    experts, _, _, rows, width = part.shape
+    slots = pltpu.VMEM((nz, experts, rows, width), part.dtype)
+    return pl.pallas_call(
+        functools.partial(collect_kernel, nz, nx),
+        out_shape=jax.ShapeDtypeStruct((experts, nz, rows, width), part.dtype),
+        in_specs=[pl.BlockSpec(memory_space=pltpu.VMEM)],
+        out_specs=pl.BlockSpec(memory_space=pltpu.VMEM),
+        scratch_shapes=[slots] * 5
+        + [pltpu.SemaphoreType.DMA((nz,))] * 8
+        + [pltpu.SemaphoreType.DMA],
+        compiler_params=pltpu.CompilerParams(collective_id=2, has_side_effects=True),
+        name="collect",
+    )(part)
 
 
 def per_device(
@@ -204,48 +420,76 @@
         * lax.rsqrt(jnp.mean(middle_wide * middle_wide, axis=1, keepdims=True) + EPS)
         * specialist_rescaling_vector[None, :]
     ).astype(jnp.bfloat16)
-    sp_count = lax.axis_size(SP)
+    nz, cores, nx = lax.axis_size("sp_0"), lax.axis_size("sp_1"), lax.axis_size("tp")
+    core = lax.axis_index("sp_1")
     local_experts = specialist_gating_matrices.shape[0]
-    experts = sp_count * local_experts
+    experts = nz * cores * local_experts
     picks = assigned_specialist_ids.shape[1]
     capacity = 2 * row_count * picks // experts
     own_ids = lax.dynamic_slice_in_dim(assigned_specialist_ids, tp_index * row_count, row_count, 0)
-    sources, position = slot_tables(own_ids, 1, row_count, experts, capacity)
-    own_position = position[0]
-    outgoing = fetch_rows(expert_input, sources).reshape(
-        sp_count, local_experts, 1, capacity, model_width
-    )
-    received = lax.all_to_all(outgoing, SP, split_axis=0, concat_axis=0, tiled=True)
-    arrived = lax.all_gather(received, "tp", axis=2, tiled=True)
+    flat_ids = own_ids.reshape(-1)
+    member = (flat_ids[:, None] == jnp.arange(experts, dtype=jnp.int32)).astype(jnp.bfloat16)
+    earlier = jnp.tril(jnp.ones((flat_ids.shape[0],) * 2, jnp.bfloat16), -1)
+    before = jnp.dot(earlier, member, preferred_element_type=jnp.float32)
+    position = jnp.sum(before * member.astype(jnp.float32), axis=1).reshape(row_count, picks)
+    lifted = jnp.exp(specialist_choice_affinity)
+    shares = cluster_chance[:, None] * lifted / jnp.sum(lifted, axis=1, keepdims=True)
+    facts = jnp.concatenate([own_ids.astype(jnp.float32), position, shares], axis=1)
+    facts = lax.all_gather(facts, "sp_1")
+    pair_ids = facts[..., :picks].astype(jnp.int32)
+    pair_places = facts[..., picks : 2 * picks].astype(jnp.int32)
+    pair_shares = facts[..., 2 * picks :]
+    per_core = cores * capacity
+    side = jnp.arange(cores, dtype=jnp.int32)[:, None, None]
+    holder = pair_ids // local_experts
+    slot = (
+        (pair_ids % local_experts * nz + holder // cores) * per_core + side * capacity + pair_places
+    )
+    slot = jnp.where(holder % cores == core, slot, -1).reshape(cores * row_count, picks)
+    pair_shares = pair_shares.reshape(cores * row_count, picks)
+    slot_count = local_experts * nz * per_core
+    slot_axis = jnp.arange(slot_count, dtype=jnp.int32)
+    pick_of = jnp.sum((slot[:, :, None] == slot_axis).astype(jnp.float32), axis=1)
+    weight_of = jnp.sum(
+        jnp.where(slot[:, :, None] == slot_axis, pair_shares[:, :, None], 0.0), axis=1
+    )
+    pair_rows = lax.all_gather(expert_input, "sp_1", axis=0, tiled=True)
+    outgoing = lax.dot_general(
+        pick_of.astype(jnp.bfloat16),
+        pair_rows,
+        (((0,), (0,)), ((), ())),
+        preferred_element_type=jnp.float32,
+    ).astype(jnp.bfloat16)
+    outgoing = outgoing.reshape(local_experts, nz, per_core, model_width)
+    arrived = dispatch(outgoing, nz, nx).reshape(local_experts, -1, model_width)
     gate_value = jnp.einsum(
-        "slqcd,ldf->slqcf", arrived, specialist_gating_matrices, preferred_element_type=jnp.float32
+        "lrd,ldf->lrf", arrived, specialist_gating_matrices, preferred_element_type=jnp.float32
     )
     up_value = jnp.einsum(
-        "slqcd,ldf->slqcf", arrived, widening_matrices, preferred_element_type=jnp.float32
+        "lrd,ldf->lrf", arrived, widening_matrices, preferred_element_type=jnp.float32
     )
     hidden = (jax.nn.silu(gate_value) * up_value).astype(jnp.bfloat16)
     partial_value = jnp.einsum(
-        "slqcf,lfd->slqcd", hidden, contracting_matrices, preferred_element_type=jnp.float32
-    )
-    width_total = summed_on_arrival(partial_value.astype(jnp.bfloat16), "tp", 2).astype(
-        jnp.bfloat16
-    )
-    returned = lax.all_to_all(width_total, SP, split_axis=0, concat_axis=0, tiled=True)
-    answers = returned.reshape(experts * capacity, model_width)
-    own_slots = own_ids.reshape(-1) * capacity + own_position
-    gathered = (
-        jnp.take(answers, own_slots, axis=0)
-        .reshape(row_count, picks, model_width)
-        .astype(jnp.float32)
-    )
-    lifted = jnp.exp(specialist_choice_affinity)
-    shares = cluster_chance[:, None] * lifted / jnp.sum(lifted, axis=1, keepdims=True)
-    return (middle_wide + jnp.sum(shares[:, :, None] * gathered, axis=1)).astype(jnp.bfloat16)
+        "lrf,lfd->lrd", hidden, contracting_matrices, preferred_element_type=jnp.float32
+    ).astype(jnp.bfloat16)
+    answers = collect(
+        partial_value.reshape(local_experts, nx, nz, per_core, model_width), nz, nx
+    ).reshape(slot_count, model_width)
+    weight_high = weight_of.astype(jnp.bfloat16)
+    weight_low = (weight_of - weight_high.astype(jnp.float32)).astype(jnp.bfloat16)
+    gathered = jnp.dot(weight_high, answers, preferred_element_type=jnp.float32) + jnp.dot(
+        weight_low, answers, preferred_element_type=jnp.float32
+    )
+    gathered = gathered.reshape(cores, row_count, model_width)
+    kept = lax.dynamic_index_in_dim(gathered, core, 0, keepdims=False)
+    given = lax.dynamic_index_in_dim(gathered, cores - 1 - core, 0, keepdims=False)
+    taken = lax.ppermute(given, "sp_1", [(0, 1), (1, 0)])
+    return (middle_wide + (kept + taken)).astype(jnp.bfloat16)
 
 
 def solution(mesh):
     finer = Mesh(
-        mesh.devices.reshape(mesh.shape["grp"], 16, 2, mesh.shape["tp"]),
+        mesh.devices.reshape(mesh.shape["grp"], mesh.shape["sp"] // 2, 2, mesh.shape["tp"]),
         ("grp", "sp_0", "sp_1", "tp"),
     )
     return jax.shard_map(

time: 420 us -> 310 us (0.74)
  Pallas kernels: 0 us -> 127 us
  blocking collectives: 169 us -> 58.3 us
  waiting for transfers between devices: 129 us -> 28.9 us
  local copies, waits for them, and re-layouts: 29.3 us -> 15.5 us
  starting transfers between devices: 30.8 us -> 19.4 us
  other arithmetic: 28.5 us -> 23 us
  matrix products: 17.5 us -> 22.8 us
    all_to_all x2 -> x0, blocking collectives: 127 us -> none  [the longest x1 76.2 us: per_device(): lax.all_to_all(outgoing, SP, split_axis=0, concat_axis=0, tiled=True)]
    pallas_call x0 -> x2, Pallas kernels: none -> 127 us  [the longest x1 66.1 us: collect(): pl.pallas_call(functools.partial(collect_kernel, nz, nx), out_shape=jax.S...]
    all_to_all x1 -> x0, waiting for transfers between devices: 55.1 us -> none  [per_device(): lax.all_to_all(width_total, SP, split_axis=0, concat_axis=0, tiled=True)]
    all_gather x1 -> x0, waiting for transfers between devices: 44 us -> none  [per_device(): arrived = lax.all_gather(received, 'tp', axis=2, tiled=True)]
    all_gather x0 -> x2, blocking collectives: none -> 16.3 us  [the longest x1 14.5 us: per_device(): pair_rows = lax.all_gather(expert_input, 'sp_1', axis=0, tiled=True)]
    all_to_all x1 -> x0, starting transfers between devices: 14.3 us -> none  [per_device(): lax.all_to_all(width_total, SP, split_axis=0, concat_axis=0, tiled=True)]
    dot_general x2 -> x6, matrix products: 11.4 us -> 17.4 us  [the longest x1 7.49 us: per_device(): jnp.einsum('lrf,lfd->lrd', hidden, contracting_matrices, preferred_elemen...]
    gather x4 -> x0, local copies, waits for them, and re-layouts: 5.68 us -> none  [the longest x2 3.1 us: per_device(): jnp.take(answers, own_slots, axis=0).reshape(row_count, picks, model_width)]
  transfers between devices with their start and end apart: 7 -> 6, of which waited for: 4 -> 3; matrix products, arithmetic and copies ran while one was open for 7% -> 10% of each run, Pallas kernels for 0% -> 0%
where the time goes in v1:
time: 310 us; the launch traced here: 309 us
  Pallas kernels  127 us (41%)
  blocking collectives  58.3 us (19%)
  waiting for transfers between devices  28.9 us (9%)
  other arithmetic  23 us (7%)
  matrix products  22.8 us (7%)
  starting transfers between devices  19.4 us (6%)
  local copies, waits for them, and re-layouts  15.5 us (5%)
  between operations  14.5 us (5%)
    pallas_call x1, Pallas kernels, collect(): pl.pallas_call(functools.partial(collect_kernel, nz, nx), out_shape=jax.S...  66.1 us
    pallas_call x1, Pallas kernels, dispatch(): pl.pallas_call(functools.partial(dispatch_kernel, nz, nx), out_shape=jax....  60.8 us
    all_gather x2, blocking collectives, carried_in(): lax.all_gather(part.astype(kind), axis)  27.5 us
    all_gather x1, waiting for transfers between devices, carried_in(): lax.all_gather(part.astype(kind), axis)  22.4 us
    unnamed x1, blocking collectives  14.5 us
    all_gather x1, blocking collectives, per_device(): pair_rows = lax.all_gather(expert_input, 'sp_1', axis=0, tiled=True)  14.5 us
    ppermute x3, starting transfers between devices, from_behind(): return lax.ppermute(x, axis, pairs)  12.5 us
    dot_general x1, matrix products, per_device(): jnp.einsum('lrf,lfd->lrd', hidden, contracting_matrices, preferred_elemen...  7.49 us
  transfers between devices with their start and end apart: 6, of which 3 were waited for; matrix products, arithmetic and copies ran while one was open for 10% of the time, Pallas kernels for 0%

profile of v1, /device:TPU:33, one launch (start us, length us, event | category | flops | bytes accessed | tf_op | source)
XLA Modules:
  0.0 309.3 jit_solution(12498736464700610997)
XLA Ops:
  7.4 5.7 %collective-permute-start.2 = (bf16[3,256]{1,0:T(4,128)(2,1)S(1)}, bf16[3,256]{1,0:T(4,128)(2,1)S(1)}, u32[]{:S(2)}, u32[]{:S(2)}) collective-permute-start(bf16[3,256]{1,0:T(4,128)(2,1)S(1)} %slice.220), channel_id=1, source_target_pairs={{0,4},{4,8},{8,12},{12,16},{16,20},{20,24},{24,28},{28,32},{32,36}... | collective-permute-start | bytes 4616 | tf_op jit(solution)/shard_map/ppermute | solution.py:52
  13.8 1.9 collective-permute-start
  15.8 1.3 slice.211
  17.0 4.8 %collective-permute-start.1 = (bf16[3,128]{1,0:T(4,128)(2,1)}, bf16[3,128]{1,0:T(4,128)(2,1)}, u32[]{:S(2)}, u32[]{:S(2)}) collective-permute-start(bf16[3,128]{1,0:T(4,128)(2,1)} %slice.211), channel_id=1, source_target_pairs={{0,4},{4,8},{8,12},{12,16},{16,20},{20,24},{24,28},{28,32},{32,36}... | collective-permute-start | bytes 2312 | tf_op jit(solution)/shard_map/ppermute | solution.py:52
  25.2 1.3 dynamic-slice
  27.3 14.5 %all-reduce = bf16[8]{0:T(256)(128)(2,1)S(1)} all-reduce(bf16[8]{0:T(256)(128)(2,1)S(1)} %dynamic-update-slice), channel_id=2, replica_groups=mesh['grp'=2,'sp_0'=16,'sp_1'=2,'tp'=4] {'sp_1'}, use_global_device_ids=true, to_apply=%add | all-reduce | flops 8 | bytes 32
  42.4 1.3 fusion.94
  46.0 1.3 multiply_divide_fusion
  51.3 5.7 %while.13 = (s32[]{:T(128)}, f32[1,4,64,128]{3,2,1,0:T(8,128)S(1)}, f32[4,1,4,64,128]{4,3,2,1,0:T(8,128)}, f32[4,1,4]{2,1,0:T(1,128)}, f32[4,1,4,64,128]{4,3,2,1,0:T(8,128)S(1)}, /*index=5*/s32[]{:T(128)}, s32[]{:T(128)}) while((s32[]{:T(128)}, f32[1,4,64,128]{3,2,1,0:T(8,128)S(1)}, f32[4,1,4,64,128]{4,3,2,1,0:T(8,128)}, ...), condition=%wide.region_2.3_spmd.clone, body=%wide.region_1.2_spmd.clone.sunk | while | flops 131075 | bytes 656016 | solution.py:107
  57.1 2.0 all-gather.1
  59.0 1.3 fusion.58
  61.9 1.8 all-gather.3
  63.8 25.5 %all_gather.28 = bf16[16,1,4]{2,1,0:T(2,128)(2,1)S(1)} all-gather(bf16[1,1,4]{2,1,0:T(2,128)(2,1)} %get-tuple-element.126), channel_id=1, replica_groups=mesh['grp'=2,'sp_0'=16,'sp_1'=2,'tp'=4] {'sp_0'}, dimensions={0}, use_global_device_ids=true | all-gather | bytes 136 | tf_op jit(solution)/shard_map/all_gather | solution.py:34
  92.1 1.0 copy.96
  95.6 22.4 %all-gather.6.cloned.1.call-done = bf16[16,1,4,64,128]{4,3,2,1,0:T(8,128)(2,1)} async-done(((bf16[1,1,4,64,128]{4,3,2,1,0:T(8,128)(2,1)}), bf16[16,1,4,64,128]{4,3,2,1,0:T(8,128)(2,1)}) %all-gather.6.cloned.1.call-update) | async-done | bytes 1048592 | tf_op jit(solution)/shard_map/all_gather | solution.py:34
  118.0 1.7 fusion.55
  119.7 1.5 fusion.5
  122.3 1.6 fusion.43
  123.9 4.2 %all-to-all-start = ((bf16[4,64,256]{2,1,0:T(8,128)(2,1)}), bf16[4,64,256]{2,1,0:T(8,128)(2,1)S(1)}, u32[]{:S(2)}, u32[]{:S(2)}) async-start(bf16[4,64,256]{2,1,0:T(8,128)(2,1)} %bitcast.53), calls=%async_computation | async-start | bytes 262144 | tf_op jit(solution)/shard_map/all_to_all | solution.py:405
  128.3 4.7 %all-to-all-done = bf16[4,64,256]{2,1,0:T(8,128)(2,1)S(1)} async-done(((bf16[4,64,256]{2,1,0:T(8,128)(2,1)}), bf16[4,64,256]{2,1,0:T(8,128)(2,1)S(1)}, u32[]{:S(2)}, u32[]{:S(2)}) %all-to-all-start) | async-done | bytes 131104 | tf_op jit(solution)/shard_map/all_to_all | solution.py:405
  133.2 3.2 %multiply_reduce_fusion = (f32[64]{0:T(128)S(1)}, f32[64,2048]{1,0:T(8,128)S(1)}) fusion(bf16[1024,2048]{1,0:T(8,128)(2,1)} %param.34, f32[64,1024]{1,0:T(8,128)S(1)} %bitcast.219, f32[1024]{0:T(1024)S(1)} %copy-done.6, f32[64]{0:T(128)S(1)} %add_rsqrt_fusion.1, bf16[64,2048]{1,0:T(8,128)(2,1)S(1)} %copy-done.2), kind=kOutput, calls=%fused_computation.33 | convolution fusion | flops 269418432 | bytes 5247488 | tf_op jit(solution)/shard_map/dot_general | solution.py:415
  136.5 14.5 %all_gather.34 = bf16[128,2048]{1,0:T(8,128)(2,1)S(1)} all-gather(bf16[64,2048]{1,0:T(8,128)(2,1)S(1)} %multiply_convert_fusion), channel_id=1, replica_groups=mesh['grp'=2,'sp_0'=16,'sp_1'=2,'tp'=4] {'sp_1'}, dimensions={0}, use_global_device_ids=true | all-gather | bytes 786432 | tf_op jit(solution)/shard_map/all_gather | solution.py:456
  151.0 1.4 convolution_convert_fusion.1
  152.4 60.8 %dispatch.1 = bf16[2,4,16,8,2048]{4,3,2,1,0:T(8,128)(2,1)} custom-call(bf16[2,16,8,2048]{3,2,1,0:T(8,128)(2,1)} %bitcast.214), custom_call_target="tpu_custom_call" | custom-call | tf_op jit(solution)/shard_map/dispatch/pallas_call | solution.py:226
  213.2 5.2 %fusion.98 = f32[2,512,256]{2,1,0:T(8,128)} fusion(bf16[2,512,2048]{2,1,0:T(8,128)(2,1)} %bitcast.211, bf16[2,2048,256]{2,1,0:T(8,128)(2,1)} %param.36), kind=kOutput, calls=%fused_computation.206 | convolution fusion | flops 1073741824 | bytes 7340032 | tf_op jit(solution)/shard_map/lrd,ldf->lrf/dot_general | solution.py:465
  218.4 7.5 %convolution_convert_fusion = bf16[2,512,2048]{2,1,0:T(8,128)(2,1)} fusion(bf16[2,256,2048]{2,1,0:T(8,128)(2,1)S(1)} %copy-done, bf16[2,512,2048]{2,1,0:T(8,128)(2,1)} %bitcast.212, bf16[2,2048,256]{2,1,0:T(8,128)(2,1)} %param.37, f32[2,512,256]{2,1,0:T(8,128)} %fusion.98), kind=kOutput, calls=%fused_computation.5 | convolution fusion | flops 2151153664 | bytes 13631488 | tf_op jit(solution)/shard_map/lrf,lfd->lrd/dot_general | solution.py:472
  225.8 66.1 %collect.1 = bf16[2,16,8,2048]{3,2,1,0:T(8,128)(2,1)} custom-call(bf16[2,4,16,8,2048]{4,3,2,1,0:T(8,128)(2,1)} %bitcast.213), custom_call_target="tpu_custom_call" | custom-call | tf_op jit(solution)/shard_map/collect/pallas_call | solution.py:344
  292.0 1.5 fusion.63
  293.5 1.5 convolution_add_fusion
  296.1 2.7 collective-permute-start.3
  298.8 1.7 collective-permute-done.3
  300.5 2.0 fusion.14
  (99 shorter events, 26.7 us)
Async XLA Ops:
  6.5 211.8 %copy-start = (bf16[2,256,2048]{2,1,0:T(8,128)(2,1)S(1)}, bf16[2,256,2048]{2,1,0:T(8,128)(2,1)}, u32[]{:S(2)}) copy-start(bf16[2,256,2048]{2,1,0:T(8,128)(2,1)} %param.38) | copy-start | bytes 6291460
  6.6 111.5 %all-gather.6.cloned.1.call-start = ((), (), s32[]{:S(2)}) async-start(), calls=%async_computation.1 | async-start | bytes 1114112 | tf_op jit(solution)/shard_map/all_gather | solution.py:34
  7.4 42.1 %collective-permute-start.2 = (bf16[3,256]{1,0:T(4,128)(2,1)S(1)}, bf16[3,256]{1,0:T(4,128)(2,1)S(1)}, u32[]{:S(2)}, u32[]{:S(2)}) collective-permute-start(bf16[3,256]{1,0:T(4,128)(2,1)S(1)} %slice.220), channel_id=1, source_target_pairs={{0,4},{4,8},{8,12},{12,16},{16,20},{20,24},{24,28},{28,32},{32,36}... | collective-permute-start | bytes 4616 | tf_op jit(solution)/shard_map/ppermute | solution.py:52
  13.8 34.7 %collective-permute-start = (bf16[3,128]{1,0:T(4,128)(2,1)S(1)}, bf16[3,128]{1,0:T(4,128)(2,1)S(1)}, u32[]{:S(2)}, u32[]{:S(2)}) collective-permute-start(bf16[3,128]{1,0:T(4,128)(2,1)S(1)} %slice.202), channel_id=1, source_target_pairs={{0,4},{4,8},{8,12},{12,16},{16,20},{20,24},{24,28},{28,32},{32,36}... | collective-permute-start | bytes 2312 | tf_op jit(solution)/shard_map/ppermute | solution.py:52
  17.0 77.5 %collective-permute-start.1 = (bf16[3,128]{1,0:T(4,128)(2,1)}, bf16[3,128]{1,0:T(4,128)(2,1)}, u32[]{:S(2)}, u32[]{:S(2)}) collective-permute-start(bf16[3,128]{1,0:T(4,128)(2,1)} %slice.211), channel_id=1, source_target_pairs={{0,4},{4,8},{8,12},{12,16},{16,20},{20,24},{24,28},{28,32},{32,36}... | collective-permute-start | bytes 2312 | tf_op jit(solution)/shard_map/ppermute | solution.py:52
  25.1 25.3 %copy-start.4 = (f32[4,1,1,4]{3,2,1,0:T(1,128)}, f32[4,1,1,4]{3,2,1,0:T(1,128)S(1)}, u32[]{:S(2)}) copy-start(f32[4,1,1,4]{3,2,1,0:T(1,128)S(1)} %get-tuple-element.96) | copy-start | bytes 196
  50.5 44.0 %copy-start.3 = (bf16[256,128]{1,0:T(8,128)(2,1)S(1)}, bf16[256,128]{1,0:T(8,128)(2,1)}, u32[]{:S(2)}) copy-start(bf16[256,128]{1,0:T(8,128)(2,1)} %param.26) | copy-start | bytes 196612
  95.2 32.9 %copy-start.7 = (s32[128,2]{0,1:T(2,128)S(1)}, s32[128,2]{0,1:T(2,128)}, u32[]{:S(2)}) copy-start(s32[128,2]{0,1:T(2,128)} %eq.52) | copy-start | bytes 3076
  95.2 32.9 %copy-start.8 = (f32[128,2]{0,1:T(2,128)S(1)}, f32[128,2]{0,1:T(2,128)}, u32[]{:S(2)}) copy-start(f32[128,2]{0,1:T(2,128)} %broadcast_in_dim.42) | copy-start | bytes 3076
  95.5 37.7 %copy-start.2 = (bf16[64,2048]{1,0:T(8,128)(2,1)S(1)}, bf16[64,2048]{1,0:T(8,128)(2,1)}, u32[]{:S(2)}) copy-start(bf16[64,2048]{1,0:T(8,128)(2,1)} %param.22) | copy-start | bytes 786436
  95.5 37.7 %copy-start.6 = (f32[1024]{0:T(1024)S(1)}, f32[1024]{0:T(1024)}, u32[]{:S(2)}) copy-start(f32[1024]{0:T(1024)} %param.33) | copy-start | bytes 12292
  121.9 14.5 %copy-start.5 = (f32[2048]{0:T(1024)S(1)}, f32[2048]{0:T(1024)}, u32[]{:S(2)}) copy-start(f32[2048]{0:T(1024)} %param.35) | copy-start | bytes 24580
  123.9 9.1 %all-to-all-start = ((bf16[4,64,256]{2,1,0:T(8,128)(2,1)}), bf16[4,64,256]{2,1,0:T(8,128)(2,1)S(1)}, u32[]{:S(2)}, u32[]{:S(2)}) async-start(bf16[4,64,256]{2,1,0:T(8,128)(2,1)} %bitcast.53), calls=%async_computation | async-start | bytes 262144 | tf_op jit(solution)/shard_map/all_to_all | solution.py:405
  295.1 1.0 copy-start.1
  296.1 4.4 %collective-permute-start.3 = (f32[64,2048]{1,0:T(8,128)S(1)}, f32[64,2048]{1,0:T(8,128)}, u32[]{:S(2)}, u32[]{:S(2)}) collective-permute-start(f32[64,2048]{1,0:T(8,128)S(1)} %dynamic-slice_bitcast_fusion), channel_id=1, source_target_pairs={{0,4},{4,0},{1,5},{5,1},{2,6},{6,2},{3,7},{7,3},{8,12},{12,8},{9,1... | collective-permute-start | bytes 1572872 | tf_op jit(solution)/shard_map/ppermute | solution.py:486
Sparse Core Ops, SparseCore 0:
  60.5 57.4 all-gather.5

commit v2 on v1

--- a/solution.py
+++ b/solution.py
@@ -8,114 +8,12 @@
 from jax.sharding import Mesh
 from jax.sharding import PartitionSpec as P
 
-HEAD_DIM = 64
-STATE = 128
-BLOCK = 64
 SP = ("sp_0", "sp_1")
 GRP_SP_TP = ("grp", "sp_0", "sp_1", "tp")
 GRP_SP = ("grp", "sp_0", "sp_1")
 
 
 EPS = 1e-06
-
-
-def filled_with(x, identity):
-    return jax.tree.map(
-        lambda part, zero: jnp.zeros_like(part) + jnp.asarray(zero, part.dtype), x, identity
-    )
-
-
-def carried_in(x, axes, combine, identity):
-    before = start = filled_with(x, identity)
-    subtotal = x
-    for axis in reversed(axes):
-        size, index = (lax.axis_size(axis), lax.axis_index(axis))
-        pieces = jax.tree.map(
-            lambda part, kind: lax.all_gather(part.astype(kind), axis),
-            subtotal,
-            (jnp.bfloat16, jnp.bfloat16),
-        )
-        inside, subtotal = (start, start)
-        for k in range(size):
-            passed = k < index
-            subtotal = combine(
-                subtotal, jax.tree.map(lambda part, own: part[k].astype(own.dtype), pieces, x)
-            )
-            inside = jax.tree.map(lambda new, old: jnp.where(passed, new, old), subtotal, inside)
-        before = combine(inside, before)
-    return before
-
-
-def from_behind(x, axis, by):
-    size = lax.axis_size(axis)
-    pairs = [(i, i + by) for i in range(size) if 0 <= i + by < size]
-    return lax.ppermute(x, axis, pairs)
-
-
-def for_sending(x):
-    return jax.tree.map(lambda a: a.astype(jnp.bfloat16) if a.dtype == jnp.float32 else a, x)
-
-
-def split_up(x, dim, size):
-    shape = x.shape
-    blocks = x.reshape(*shape[:dim], size, shape[dim] // size, *shape[dim + 1 :])
-    return jnp.moveaxis(blocks, dim, 0)
-
-
-def summed_on_arrival(x, axis, dim):
-    size = lax.axis_size(axis)
-    blocks = lax.all_to_all(split_up(x, dim, size), axis, 0, 0, tiled=True)
-    return jnp.sum(blocks.astype(jnp.float32), axis=0)
-
-
-def causal_conv(signal, earlier, weights):
-    kernel_len = weights.shape[0]
-    length = signal.shape[0]
-    joined = jnp.concatenate([earlier, signal], axis=0).astype(jnp.float32)
-    accumulated = jnp.zeros((length, signal.shape[1]), jnp.float32)
-    for offset in range(kernel_len):
-        accumulated = accumulated + weights[offset][None, :] * joined[offset : offset + length]
-    return jax.nn.silu(accumulated)
-
-
-def link_states(earlier, later):
-    return (earlier[0] * later[0], earlier[1] * later[0][..., None, None] + later[1])
-
-
-def device_states(scaled_in, log_attenuation, keys_b, queries_c, groups_here):
-    length = scaled_in.shape[0]
-    blocks = length // BLOCK
-    per_group = scaled_in.shape[1] // groups_here
-    scaled_in = scaled_in.reshape(blocks, BLOCK, groups_here, per_group, HEAD_DIM)
-    log_attenuation = log_attenuation.reshape(blocks, BLOCK, groups_here, per_group)
-    keys_b = keys_b.reshape(blocks, BLOCK, groups_here, STATE)
-    queries_c = queries_c.reshape(blocks, BLOCK, groups_here, STATE)
-    running = jnp.cumsum(log_attenuation, axis=1)
-    lower_mask = jnp.tril(jnp.ones((BLOCK, BLOCK), dtype=bool))
-    between = running[:, :, None] - running[:, None, :]
-    decays = jnp.exp(jnp.where(lower_mask[None, :, :, None, None], between, -jnp.inf))
-    scores = jnp.einsum("blgn,bsgn->blsg", queries_c, keys_b)
-    inside = jnp.einsum("blsg,blsgr,bsgrp->blgrp", scores, decays, scaled_in)
-    totals = running[:, -1]
-    remain = jnp.exp(totals[:, None] - running)
-    block_states = jnp.einsum("bsgn,bsgr,bsgrp->bgrpn", keys_b, remain, scaled_in)
-
-    def advance(carried, pieces):
-        return (carried * jnp.exp(pieces[1])[..., None, None] + pieces[0], carried)
-
-    initial = jnp.zeros(block_states.shape[1:], jnp.float32)
-    own_state, entering = lax.scan(advance, initial, (block_states, totals))
-    own_decay = jnp.exp(jnp.sum(totals, axis=0))
-    _, incoming = carried_in(
-        (own_decay, own_state),
-        SP,
-        link_states,
-        (jnp.ones_like(own_decay), jnp.zeros_like(own_state)),
-    )
-    preceding = jnp.exp(jnp.cumsum(totals, axis=0) - totals)
-    entering = entering + preceding[..., None, None] * incoming[None]
-    outside = jnp.einsum("blgn,bgrpn,blgr->blgrp", queries_c, entering, jnp.exp(running))
-    return (inside + outside).reshape(length, -1)
 
 
 def hop(step):
@@ -352,6 +250,486 @@
         compiler_params=pltpu.CompilerParams(collective_id=2, has_side_effects=True),
         name="collect",
     )(part)
+
+
+QUAD = 4
+TAIL = 16
+
+
+def greet_all(nz, nx):
+    z, c, x = lax.axis_index("sp_0"), lax.axis_index("sp_1"), lax.axis_index("tp")
+    barrier = pltpu.get_barrier_semaphore()
+
+    def along_z(k, carry):
+        pl.semaphore_signal(barrier, inc=1, device_id={"sp_0": lax.rem(z + k, nz)})
+        return carry
+
+    def along_x(k, carry):
+        pl.semaphore_signal(barrier, inc=1, device_id={"tp": lax.rem(x + k, nx)})
+        return carry
+
+    lax.fori_loop(1, nz, along_z, 0)
+    lax.fori_loop(1, nx, along_x, 0)
+    pl.semaphore_signal(barrier, inc=1, device_id={"sp_1": 1 - c})
+    pl.semaphore_signal(
+        barrier, inc=1, device_id={"sp_0": lax.rem(z + nz - 1 + 2 * c, nz), "sp_1": 1 - c}
+    )
+    pl.semaphore_wait(barrier, nz + nx)
+
+
+def silu(v):
+    return v * jax.nn.sigmoid(v)
+
+
+def exact_dot(a, b):
+    return jnp.dot(a, b, preferred_element_type=jnp.float32, precision=lax.Precision.HIGHEST)
+
+
+def packed(state, decays):
+    lanes = state.shape[1]
+    row = lax.broadcasted_iota(jnp.int32, (TAIL, lanes), 0)
+    tail = jnp.zeros((TAIL, lanes), jnp.float32)
+    for h, decay in enumerate(decays):
+        wide = jnp.broadcast_to(decay, (TAIL, lanes))
+        high = wide.astype(jnp.bfloat16).astype(jnp.float32)
+        tail = jnp.where(row == h, high, tail)
+        tail = jnp.where(row == TAIL // 2 + h, wide - high, tail)
+    return jnp.concatenate([state.astype(jnp.bfloat16), tail.astype(jnp.bfloat16)], axis=0)
+
+
+def unpacked(message, heads):
+    rows = message.shape[0] - TAIL
+    state = message[:rows].astype(jnp.float32)
+    tail = message[rows:].astype(jnp.float32)
+    half = TAIL // 2
+    return state, [tail[h : h + 1, 0:1] + tail[half + h : half + h + 1, 0:1] for h in range(heads)]
+
+
+def per_row(decays, rows, lanes):
+    each = rows // len(decays)
+    return jnp.concatenate([jnp.broadcast_to(d, (each, lanes)) for d in decays], axis=0)
+
+
+def followed(earlier, later):
+    (state_a, decay_a), (state_b, decay_b) = earlier, later
+    state = state_a * per_row(decay_b, *state_a.shape) + state_b
+    return state, [a * b for a, b in zip(decay_a, decay_b)]
+
+
+def chosen(flag, one, other):
+    return jnp.where(flag, one[0], other[0]), [
+        jnp.where(flag, a, b) for a, b in zip(one[1], other[1])
+    ]
+
+
+def front_kernel(
+    nz,
+    nx,
+    capacity,
+    xs_ref,
+    gate_ref,
+    keys_ref,
+    queries_ref,
+    raw_ref,
+    extra_ref,
+    rate_ref,
+    taps_ref,
+    gain_ref,
+    blend_hbm,
+    carry_ref,
+    gain2_ref,
+    ids_ref,
+    affinity_ref,
+    chance_ref,
+    outgoing_ref,
+    middle_ref,
+    weight_ref,
+    halo,
+    joined,
+    pair_out,
+    pair_in,
+    quad_out,
+    quad_in,
+    far_out,
+    far_in,
+    half_out,
+    half_in,
+    gated_out,
+    gated_in,
+    facts,
+    rows,
+    blend,
+    blend_sem,
+    halo_s,
+    halo_r,
+    pair_s,
+    pair_r,
+    quad_s,
+    quad_r,
+    far_s,
+    far_r,
+    gated_s,
+    gated_r,
+):
+    z, c, x = lax.axis_index("sp_0"), lax.axis_index("sp_1"), lax.axis_index("tp")
+    length, width_x = xs_ref.shape
+    state_width = keys_ref.shape[1]
+    heads = raw_ref.shape[1]
+    head_dim = width_x // heads
+    half_heads = heads // 2
+    half_rows = width_x // 2
+    place, quad = lax.rem(z, QUAD), z // QUAD
+    quads = nz // QUAD
+    f32, bf16 = jnp.float32, jnp.bfloat16
+    partner = {"sp_1": 1 - c}
+    load = pltpu.make_async_copy(blend_hbm, blend, blend_sem)
+    load.start()
+
+    count, picks = ids_ref.shape[0] // nx, ids_ref.shape[1]
+    local_experts = outgoing_ref.shape[0]
+    experts = nz * 2 * local_experts
+    ids = ids_ref[pl.ds(pl.multiple_of(x * count, count), count), :]
+    expert_axis = lax.broadcasted_iota(jnp.int32, (count, experts), 1)
+    member = [(ids[:, k : k + 1] == expert_axis).astype(f32) for k in range(picks)]
+    row_axis = lax.broadcasted_iota(jnp.int32, (count, count), 0)
+    column_axis = lax.broadcasted_iota(jnp.int32, (count, count), 1)
+    earlier = (row_axis > column_axis).astype(bf16)
+    before = jnp.dot(earlier, sum(member).astype(bf16), preferred_element_type=f32)
+    lifted = jnp.exp(affinity_ref[...])
+    shares = chance_ref[...] * lifted / jnp.sum(lifted, axis=1, keepdims=True)
+    lane = lax.broadcasted_iota(jnp.int32, (count, facts.shape[2]), 1)
+    noted = jnp.zeros((count, facts.shape[2]), f32)
+    for k in range(picks):
+        position = jnp.sum(before * member[k], axis=1, keepdims=True)
+        expert = ids[:, k : k + 1]
+        holder = lax.div(expert, local_experts)
+        slot = (
+            (lax.rem(expert, local_experts) * nz + lax.div(holder, 2)) * 2 + c
+        ) * capacity + position.astype(jnp.int32)
+        for core in range(2):
+            there = jnp.where(lax.rem(holder, 2) == core, slot, -1).astype(f32)
+            noted = jnp.where(lane == core * picks + k, there, noted)
+        noted = jnp.where(lane == 2 * picks + k, shares[:, k : k + 1], noted)
+    facts[c] = noted
+
+    greet_all(nz, nx)
+    rim = halo.shape[0]
+    after = {"sp_0": lax.rem(z + c, nz), "sp_1": 1 - c}
+    edges = []
+    start = 0
+    for n, ref in enumerate((xs_ref, keys_ref, queries_ref)):
+        columns = pl.ds(start, ref.shape[1])
+        edges.append(
+            pltpu.make_async_remote_copy(
+                ref.at[pl.ds(length - rim, rim)],
+                halo.at[:, columns],
+                halo_s.at[n],
+                halo_r.at[n],
+                device_id=after,
+            )
+        )
+        start += ref.shape[1]
+    for edge in edges:
+        edge.start()
+    facts_copy = pltpu.make_async_remote_copy(
+        facts.at[c], facts.at[c], pair_s.at[0], pair_r.at[0], device_id=partner
+    )
+    facts_copy.start()
+
+    stride = jnp.maximum(raw_ref[...], 0.0) + jnp.log1p(jnp.exp(-jnp.abs(raw_ref[...])))
+    log_decay = extra_ref[...] - rate_ref[...] * stride
+    lane = lax.broadcasted_iota(jnp.int32, (length, 128), 1)
+    padded = jnp.zeros((length, 128), f32)
+    for h in range(heads):
+        padded = jnp.where(lane == h, log_decay[:, h : h + 1], padded)
+    t_axis = lax.broadcasted_iota(jnp.int32, (length, length), 0)
+    s_axis = lax.broadcasted_iota(jnp.int32, (length, length), 1)
+    causal = t_axis >= s_axis
+    running = exact_dot(causal.astype(f32), padded)
+    running_row = running.T
+    final = running[length - 1 : length, :]
+
+    start = 0
+    for ref in (xs_ref, keys_ref, queries_ref):
+        joined[rim:, start : start + ref.shape[1]] = ref[...].astype(f32)
+        start += ref.shape[1]
+    for edge in edges:
+        edge.wait_recv()
+    joined[:rim, :] = jnp.where(z + c > 0, halo[...].astype(f32), 0.0)
+    kernel_len = taps_ref.shape[0]
+    convolved = taps_ref[0:1, :] * joined[rim - kernel_len + 1 : rim - kernel_len + 1 + length, :]
+    for tap in range(1, kernel_len):
+        first = rim - kernel_len + 1 + tap
+        convolved = convolved + taps_ref[tap : tap + 1, :] * joined[first : first + length, :]
+    convolved = silu(convolved)
+    inputs_x = convolved[:, :width_x]
+    keys_b = convolved[:, width_x : width_x + state_width].astype(bf16)
+    queries_c = convolved[:, width_x + state_width :].astype(bf16)
+
+    scaled = [
+        inputs_x[:, h * head_dim : (h + 1) * head_dim] * stride[:, h : h + 1] for h in range(heads)
+    ]
+    remaining = jnp.concatenate(
+        [scaled[h] * jnp.exp(final[:, h : h + 1] - running[:, h : h + 1]) for h in range(heads)],
+        axis=1,
+    ).astype(bf16)
+    own_state = lax.dot_general(
+        remaining, keys_b, (((0,), (0,)), ((), ())), preferred_element_type=f32
+    )
+    pair_out[...] = packed(own_state, [jnp.exp(final[:, h : h + 1]) for h in range(heads)])
+    pair_copy = pltpu.make_async_remote_copy(
+        pair_out, pair_in, pair_s.at[1], pair_r.at[1], device_id=partner
+    )
+    pair_copy.start()
+
+    scores = lax.dot_general(
+        queries_c, keys_b, (((1,), (1,)), ((), ())), preferred_element_type=f32
+    )
+    inside = []
+    for h in range(heads):
+        between = running[:, h : h + 1] - running_row[h : h + 1, :]
+        decays = jnp.exp(jnp.where(causal, between, -1e30))
+        inside.append(
+            jnp.dot(
+                (scores * decays).astype(bf16), scaled[h].astype(bf16), preferred_element_type=f32
+            )
+        )
+
+    pair_copy.wait_recv()
+
+    def half_of(ref):
+        state, decays = unpacked(ref[...], heads)
+        return (
+            jnp.where(c == 0, state[:half_rows], state[half_rows:]),
+            [jnp.where(c == 0, decays[j], decays[half_heads + j]) for j in range(half_heads)],
+        )
+
+    ours, theirs = half_of(pair_out), half_of(pair_in)
+    lower, upper = chosen(c == 0, ours, theirs), chosen(c == 0, theirs, ours)
+    chip = followed(lower, upper)
+    quad_out[...] = packed(*chip)
+
+    def quad_send(k):
+        to = quad * QUAD + lax.rem(place + k, QUAD)
+        return pltpu.make_async_remote_copy(
+            quad_out, quad_in.at[place], quad_s.at[k], quad_r.at[k], device_id={"sp_0": to}
+        )
+
+    def quad_arrival(k):
+        return pltpu.make_async_remote_copy(
+            quad_out,
+            quad_in.at[lax.rem(place + QUAD - k, QUAD)],
+            quad_s.at[k],
+            quad_r.at[k],
+            device_id={"sp_0": lax.rem(z + 1, nz)},
+        )
+
+    for k in range(1, QUAD):
+        quad_send(k).start()
+    quad_in[place] = quad_out[...]
+    for k in range(1, QUAD):
+        quad_arrival(k).wait_recv()
+    nothing = (jnp.zeros_like(chip[0]), [jnp.ones_like(d) for d in chip[1]])
+    whole, inner = nothing, nothing
+    for k in range(QUAD):
+        inner = chosen(place == k, whole, inner)
+        whole = followed(whole, unpacked(quad_in[k], half_heads))
+    far_out[...] = packed(*whole)
+
+    def far_send(k):
+        return pltpu.make_async_remote_copy(
+            far_out,
+            far_in.at[k],
+            far_s.at[k],
+            far_r.at[k],
+            device_id={"sp_0": lax.rem(z + k * QUAD, nz)},
+        )
+
+    for k in range(1, quads):
+
+        @pl.when(quad + k < quads)
+        def _(k=k):
+            far_send(k).start()
+
+    far_in[0] = jnp.zeros_like(far_out)
+    for k in range(1, quads):
+
+        @pl.when(quad >= k)
+        def _(k=k):
+            far_send(k).wait_recv()
+
+        @pl.when(quad < k)
+        def _(k=k):
+            far_in[k] = jnp.zeros_like(far_out)
+
+    incoming = nothing
+    for k in reversed(range(1, quads)):
+        incoming = followed(incoming, unpacked(far_in[k], half_heads))
+    incoming = followed(incoming, inner)
+    incoming_low = incoming[0]
+    incoming_high = followed(incoming, lower)[0]
+    half_out[...] = jnp.where(c == 0, incoming_high, incoming_low).astype(bf16)
+    half_copy = pltpu.make_async_remote_copy(
+        half_out, half_in, pair_s.at[2], pair_r.at[2], device_id=partner
+    )
+    half_copy.start()
+    kept = jnp.where(c == 0, incoming_low, incoming_high).astype(bf16)
+    modulation = silu(gate_ref[...].astype(f32))
+    half_copy.wait_recv()
+    sent_in = half_in[...]
+    entering = jnp.concatenate(
+        [jnp.where(c == 0, kept, sent_in), jnp.where(c == 0, sent_in, kept)], axis=0
+    )
+    outside = lax.dot_general(
+        queries_c, entering, (((1,), (1,)), ((), ())), preferred_element_type=f32
+    )
+    mixed = jnp.concatenate(
+        [
+            inside[h]
+            + outside[:, h * head_dim : (h + 1) * head_dim] * jnp.exp(running[:, h : h + 1])
+            for h in range(heads)
+        ],
+        axis=1,
+    )
+    gated_out[...] = (mixed * modulation).astype(bf16).reshape(gated_out.shape)
+
+    def gated_send(k):
+        to = lax.rem(x + k, nx)
+        return pltpu.make_async_remote_copy(
+            gated_out.at[to], gated_in.at[x], gated_s.at[k], gated_r.at[k], device_id={"tp": to}
+        )
+
+    for k in range(1, nx):
+        gated_send(k).start()
+    gated_in[x] = gated_out[x]
+    facts_arrival = pltpu.make_async_remote_copy(
+        facts.at[1 - c], facts.at[1 - c], pair_s.at[0], pair_r.at[0], device_id=partner
+    )
+    facts_arrival.wait_recv()
+    slot_count = weight_ref.shape[1]
+    slot_axis = lax.broadcasted_iota(jnp.int32, (2 * count, slot_count), 1).astype(f32)
+    known = jnp.concatenate([facts[0], facts[1]], axis=0)
+    picked = jnp.zeros((2 * count, slot_count), f32)
+    weight = jnp.zeros((2 * count, slot_count), f32)
+    for k in range(picks):
+        slot = jnp.where(c == 0, known[:, k : k + 1], known[:, picks + k : picks + k + 1])
+        hit = slot == slot_axis
+        picked = jnp.where(hit, 1.0, picked)
+        weight = jnp.where(hit, known[:, 2 * picks + k : 2 * picks + k + 1], weight)
+    weight_ref[...] = weight
+    for k in range(1, nx):
+        pltpu.make_async_remote_copy(
+            gated_out.at[x],
+            gated_in.at[lax.rem(x + nx - k, nx)],
+            gated_s.at[k],
+            gated_r.at[k],
+            device_id={"tp": lax.rem(x + k, nx)},
+        ).wait_recv()
+    own_rows = jnp.concatenate([gated_in[k] for k in range(nx)], axis=1).astype(f32)
+    normed = (
+        own_rows
+        * lax.rsqrt(jnp.mean(own_rows * own_rows, axis=1, keepdims=True) + EPS)
+        * gain_ref[...]
+    ).astype(bf16)
+    load.wait()
+    middle = (
+        carry_ref[...].astype(f32) + jnp.dot(normed, blend[...], preferred_element_type=f32)
+    ).astype(bf16)
+    middle_ref[...] = middle
+    wide = middle.astype(f32)
+    rows[c] = (
+        wide
+        * lax.rsqrt(jnp.mean(wide * wide, axis=1, keepdims=True) + EPS)
+        * gain2_ref[...]
+    ).astype(bf16)
+    rows_copy = pltpu.make_async_remote_copy(
+        rows.at[c], rows.at[c], pair_s.at[3], pair_r.at[3], device_id=partner
+    )
+    rows_copy.start()
+    pltpu.make_async_remote_copy(
+        rows.at[1 - c], rows.at[1 - c], pair_s.at[3], pair_r.at[3], device_id=partner
+    ).wait_recv()
+    outgoing_ref[...] = (
+        lax.dot_general(
+            picked.astype(bf16),
+            jnp.concatenate([rows[0], rows[1]], axis=0),
+            (((0,), (0,)), ((), ())),
+            preferred_element_type=f32,
+        )
+        .astype(bf16)
+        .reshape(outgoing_ref.shape)
+    )
+
+    for edge in edges:
+        edge.wait_send()
+    facts_copy.wait_send()
+    pair_copy.wait_send()
+    half_copy.wait_send()
+    rows_copy.wait_send()
+    for k in range(1, QUAD):
+        quad_send(k).wait_send()
+    for k in range(1, quads):
+
+        @pl.when(quad + k < quads)
+        def _(k=k):
+            far_send(k).wait_send()
+
+    for k in range(1, nx):
+        gated_send(k).wait_send()
+
+
+def front(nz, nx, local_experts, capacity, *arrays):
+    xs, _, keys, queries, raw = arrays[:5]
+    blend, carry = arrays[9:11]
+    count, width = carry.shape
+    slots = local_experts * nz * 2 * capacity
+    channels = xs.shape[1]
+    total = channels + keys.shape[1] + queries.shape[1]
+    rim = 8
+    states = keys.shape[1]
+    bf16 = jnp.bfloat16
+    vmem = pl.BlockSpec(memory_space=pltpu.VMEM)
+    half = channels // 2
+    return pl.pallas_call(
+        functools.partial(front_kernel, nz, nx, capacity),
+        out_shape=(
+            jax.ShapeDtypeStruct((local_experts, nz, 2 * capacity, width), bf16),
+            jax.ShapeDtypeStruct((count, width), bf16),
+            jax.ShapeDtypeStruct((2 * count, slots), jnp.float32),
+        ),
+        in_specs=[vmem] * 9 + [pl.BlockSpec(memory_space=pl.ANY)] + [vmem] * 5,
+        out_specs=(vmem, vmem, vmem),
+        scratch_shapes=[
+            pltpu.VMEM((rim, total), bf16),
+            pltpu.VMEM((rim + xs.shape[0], total), jnp.float32),
+            pltpu.VMEM((channels + TAIL, states), bf16),
+            pltpu.VMEM((channels + TAIL, states), bf16),
+            pltpu.VMEM((half + TAIL, states), bf16),
+            pltpu.VMEM((QUAD, half + TAIL, states), bf16),
+            pltpu.VMEM((half + TAIL, states), bf16),
+            pltpu.VMEM((nz // QUAD, half + TAIL, states), bf16),
+            pltpu.VMEM((half, states), bf16),
+            pltpu.VMEM((half, states), bf16),
+            pltpu.VMEM((nx, count, channels), bf16),
+            pltpu.VMEM((nx, count, channels), bf16),
+            pltpu.VMEM((2, count, 128), jnp.float32),
+            pltpu.VMEM((2, count, width), bf16),
+            pltpu.VMEM(blend.shape, bf16),
+            pltpu.SemaphoreType.DMA,
+            pltpu.SemaphoreType.DMA((3,)),
+            pltpu.SemaphoreType.DMA((3,)),
+            pltpu.SemaphoreType.DMA((4,)),
+            pltpu.SemaphoreType.DMA((4,)),
+            pltpu.SemaphoreType.DMA((QUAD,)),
+            pltpu.SemaphoreType.DMA((QUAD,)),
+            pltpu.SemaphoreType.DMA((nz // QUAD,)),
+            pltpu.SemaphoreType.DMA((nz // QUAD,)),
+            pltpu.SemaphoreType.DMA((nx,)),
+            pltpu.SemaphoreType.DMA((nx,)),
+        ],
+        compiler_params=pltpu.CompilerParams(collective_id=3, has_side_effects=True),
+        name="front",
+    )(*arrays)
 
 
 def per_device(
@@ -376,91 +754,40 @@
     specialist_choice_affinity,
     cluster_chance,
 ):
-    length = channel_source_entries.shape[0]
-    row_count = carryover_vector.shape[0]
-    model_width = carryover_vector.shape[1]
-    heads_here = channel_fading_rate.shape[0]
-    groups_here = entering_basis_matrix.shape[1] // STATE
-    tp_index = lax.axis_index("tp")
-    rim_rows = channel_source_kernel.shape[0] - 1
-    neighbours = from_behind(
-        (
-            channel_source_entries[length - rim_rows :],
-            entering_basis_matrix[length - rim_rows :],
-            readout_basis_matrix[length - rim_rows :],
-        ),
-        SP,
-        1,
-    )
-    inputs_x = causal_conv(channel_source_entries, neighbours[0], channel_source_kernel)
-    keys_b = causal_conv(entering_basis_matrix, neighbours[1], entering_basis_kernel)
-    queries_c = causal_conv(readout_basis_matrix, neighbours[2], readout_basis_kernel)
-    channel_stride_amount = jax.nn.softplus(raw_stride_amount)
-    log_attenuation = extra_log_attenuation - channel_fading_rate[None, :] * channel_stride_amount
-    heads_x = inputs_x.reshape(length, heads_here, HEAD_DIM)
-    mixed = device_states(
-        heads_x * channel_stride_amount[:, :, None], log_attenuation, keys_b, queries_c, groups_here
-    )
-    gated = mixed * jax.nn.silu(final_modulation_vector.astype(jnp.float32))
-    own_rows = lax.all_to_all(
-        for_sending(gated), "tp", split_axis=0, concat_axis=1, tiled=True
-    ).astype(gated.dtype)
-    normed = (
-        own_rows
-        * lax.rsqrt(jnp.mean(own_rows * own_rows, axis=1, keepdims=True) + EPS)
-        * modulated_rescaling_vector[None, :]
-    ).astype(jnp.bfloat16)
-    middle = (
-        carryover_vector.astype(jnp.float32)
-        + jnp.dot(normed, blender_final_matrix, preferred_element_type=jnp.float32)
-    ).astype(jnp.bfloat16)
-    middle_wide = middle.astype(jnp.float32)
-    expert_input = (
-        middle_wide
-        * lax.rsqrt(jnp.mean(middle_wide * middle_wide, axis=1, keepdims=True) + EPS)
-        * specialist_rescaling_vector[None, :]
-    ).astype(jnp.bfloat16)
     nz, cores, nx = lax.axis_size("sp_0"), lax.axis_size("sp_1"), lax.axis_size("tp")
     core = lax.axis_index("sp_1")
+    row_count, model_width = carryover_vector.shape
     local_experts = specialist_gating_matrices.shape[0]
     experts = nz * cores * local_experts
     picks = assigned_specialist_ids.shape[1]
     capacity = 2 * row_count * picks // experts
-    own_ids = lax.dynamic_slice_in_dim(assigned_specialist_ids, tp_index * row_count, row_count, 0)
-    flat_ids = own_ids.reshape(-1)
-    member = (flat_ids[:, None] == jnp.arange(experts, dtype=jnp.int32)).astype(jnp.bfloat16)
-    earlier = jnp.tril(jnp.ones((flat_ids.shape[0],) * 2, jnp.bfloat16), -1)
-    before = jnp.dot(earlier, member, preferred_element_type=jnp.float32)
-    position = jnp.sum(before * member.astype(jnp.float32), axis=1).reshape(row_count, picks)
-    lifted = jnp.exp(specialist_choice_affinity)
-    shares = cluster_chance[:, None] * lifted / jnp.sum(lifted, axis=1, keepdims=True)
-    facts = jnp.concatenate([own_ids.astype(jnp.float32), position, shares], axis=1)
-    facts = lax.all_gather(facts, "sp_1")
-    pair_ids = facts[..., :picks].astype(jnp.int32)
-    pair_places = facts[..., picks : 2 * picks].astype(jnp.int32)
-    pair_shares = facts[..., 2 * picks :]
     per_core = cores * capacity
-    side = jnp.arange(cores, dtype=jnp.int32)[:, None, None]
-    holder = pair_ids // local_experts
-    slot = (
-        (pair_ids % local_experts * nz + holder // cores) * per_core + side * capacity + pair_places
-    )
-    slot = jnp.where(holder % cores == core, slot, -1).reshape(cores * row_count, picks)
-    pair_shares = pair_shares.reshape(cores * row_count, picks)
-    slot_count = local_experts * nz * per_core
-    slot_axis = jnp.arange(slot_count, dtype=jnp.int32)
-    pick_of = jnp.sum((slot[:, :, None] == slot_axis).astype(jnp.float32), axis=1)
-    weight_of = jnp.sum(
-        jnp.where(slot[:, :, None] == slot_axis, pair_shares[:, :, None], 0.0), axis=1
-    )
-    pair_rows = lax.all_gather(expert_input, "sp_1", axis=0, tiled=True)
-    outgoing = lax.dot_general(
-        pick_of.astype(jnp.bfloat16),
-        pair_rows,
-        (((0,), (0,)), ((), ())),
-        preferred_element_type=jnp.float32,
-    ).astype(jnp.bfloat16)
-    outgoing = outgoing.reshape(local_experts, nz, per_core, model_width)
+    taps = jnp.concatenate(
+        [channel_source_kernel, entering_basis_kernel, readout_basis_kernel], axis=1
+    )
+    outgoing, middle, weight_of = front(
+        nz,
+        nx,
+        local_experts,
+        capacity,
+        channel_source_entries,
+        final_modulation_vector,
+        entering_basis_matrix,
+        readout_basis_matrix,
+        raw_stride_amount,
+        extra_log_attenuation,
+        channel_fading_rate[None, :],
+        taps,
+        modulated_rescaling_vector[None, :],
+        blender_final_matrix,
+        carryover_vector,
+        specialist_rescaling_vector[None, :],
+        assigned_specialist_ids,
+        specialist_choice_affinity,
+        cluster_chance[:, None],
+    )
+    middle_wide = middle.astype(jnp.float32)
+    slot_count = weight_of.shape[1]
     arrived = dispatch(outgoing, nz, nx).reshape(local_experts, -1, model_width)
     gate_value = jnp.einsum(
         "lrd,ldf->lrf", arrived, specialist_gating_matrices, preferred_element_type=jnp.float32

time: 310 us -> 215 us (0.69)
  blocking collectives: 58.3 us -> 0 us
  Pallas kernels: 127 us -> 185 us
  waiting for transfers between devices: 28.9 us -> 1.88 us
  other arithmetic: 23 us -> 3.13 us
  starting transfers between devices: 19.4 us -> 2.69 us
  between operations: 14.5 us -> 0.1 us
  matrix products: 22.8 us -> 13.3 us
  local copies, waits for them, and re-layouts: 15.5 us -> 8.15 us
    pallas_call x0 -> x1, Pallas kernels: none -> 45.4 us  [front(): pl.pallas_call(functools.partial(front_kernel, nz, nx, capacity), out_sha...]
    all_gather x4 -> x0, blocking collectives: 43.8 us -> none  [the longest x2 27.5 us: carried_in(): lax.all_gather(part.astype(kind), axis)]
    all_gather x1 -> x0, waiting for transfers between devices: 22.4 us -> none  [carried_in(): lax.all_gather(part.astype(kind), axis)]
    unnamed x1 -> x0, blocking collectives: 14.5 us -> none
    ppermute x3 -> x0, starting transfers between devices: 12.5 us -> none  [from_behind(): return lax.ppermute(x, axis, pairs)]
    pallas_call x1, Pallas kernels: 60.8 us -> 72.9 us  [dispatch(): pl.pallas_call(functools.partial(dispatch_kernel, nz, nx), out_shape=jax....]
    convert_element_type x12 -> x0, other arithmetic: 8.78 us -> none  [the longest x3 2.48 us: causal_conv(): joined = jnp.concatenate([earlier, signal], axis=0).astype(jnp.float32)]
    dot_general x7 -> x0, matrix products: 7.04 us -> none  [the longest x1 3.21 us: per_device(): jnp.dot(normed, blender_final_matrix, preferred_element_type=jnp.float32)]
  transfers between devices with their start and end apart: 6 -> 1, of which waited for: 3 -> 1; matrix products, arithmetic and copies ran while one was open for 10% -> 0% of each run, Pallas kernels for 0% -> 0%
where the time goes in v2:
time: 215 us; the launch traced here: 214 us
  Pallas kernels  185 us (86%)
  matrix products  13.3 us (6%)
  local copies, waits for them, and re-layouts  8.15 us (4%)
  other arithmetic  3.13 us (1%)
  starting transfers between devices  2.69 us (1%)
    pallas_call x1, Pallas kernels, dispatch(): pl.pallas_call(functools.partial(dispatch_kernel, nz, nx), out_shape=jax....  72.9 us
    pallas_call x1, Pallas kernels, collect(): pl.pallas_call(functools.partial(collect_kernel, nz, nx), out_shape=jax.S...  66.7 us
    pallas_call x1, Pallas kernels, front(): pl.pallas_call(functools.partial(front_kernel, nz, nx, capacity), out_sha...  45.4 us
    dot_general x1, matrix products, per_device(): jnp.einsum('lrf,lfd->lrd', hidden, contracting_matrices, preferred_elemen...  7.31 us
    unnamed x12, local copies, waits for them, and re-layouts  5.96 us
  transfers between devices with their start and end apart: 1, of which 1 were waited for; matrix products, arithmetic and copies ran while one was open for 0% of the time, Pallas kernels for 0%

profile of v2, /device:TPU:33, one launch (start us, length us, event | category | flops | bytes accessed | tf_op | source)
XLA Modules:
  0.0 214.4 jit_solution(2637379590995519111)
XLA Ops:
  0.0 0.0 copy-start
  0.0 1.6 copy.21.raw_ref
  1.6 1.5 copy.22.extra_ref
  3.1 1.5 copy.23.ids_ref
  4.6 1.4 copy.24.affinity_ref
  6.0 1.4 copy.25.chance_ref
  7.3 1.3 pad_maximum_fusion.taps_ref
  8.6 45.4 %front.1 = (bf16[2,16,8,2048]{3,2,1,0:T(8,128)(2,1)}, bf16[64,2048]{1,0:T(8,128)(2,1)}, f32[128,256]{1,0:T(8,128)}) custom-call(bf16[256,256]{1,0:T(8,128)(2,1)} %xs_ref.1, bf16[256,256]{1,0:T(8,128)(2,1)} %gate_ref.1, bf16[256,128]{1,0:T(8,128)(2,1)} %keys_ref.1, bf16[256,128]{1,0:T(8,128)(2,1)} %queries_ref.1, f32[256,4]{1,0:T(8,128)} %copy.21.raw_ref, ...), custom_call_target="tpu_custom_call" | custom-call | tf_op jit(solution)/shard_map/front/pallas_call | solution.py:693
  54.1 72.9 %dispatch.1 = bf16[2,4,16,8,2048]{4,3,2,1,0:T(8,128)(2,1)} custom-call(bf16[2,16,8,2048]{3,2,1,0:T(8,128)(2,1)} %get-tuple-element.10.src), custom_call_target="tpu_custom_call" | custom-call | tf_op jit(solution)/shard_map/dispatch/pallas_call | solution.py:124
  127.0 4.1 %fusion.13 = f32[2,512,256]{2,1,0:T(8,128)S(1)} fusion(bf16[2,512,2048]{2,1,0:T(8,128)(2,1)} %bitcast.25, bf16[2,2048,256]{2,1,0:T(8,128)(2,1)} %param.34), kind=kOutput, calls=%fused_computation.20 | convolution fusion | flops 1073741824 | bytes 7340032 | tf_op jit(solution)/shard_map/lrd,ldf->lrf/dot_general | solution.py:792
  131.1 0.0 copy-done
  131.1 7.3 %convolution_convert_fusion = bf16[2,512,2048]{2,1,0:T(8,128)(2,1)} fusion(bf16[2,256,2048]{2,1,0:T(8,128)(2,1)S(1)} %copy-done, bf16[2,512,2048]{2,1,0:T(8,128)(2,1)} %bitcast.26, bf16[2,2048,256]{2,1,0:T(8,128)(2,1)} %param.35, f32[2,512,256]{2,1,0:T(8,128)S(1)} %fusion.13), kind=kOutput, calls=%fused_computation | convolution fusion | flops 2151153664 | bytes 13631488 | tf_op jit(solution)/shard_map/lrf,lfd->lrd/dot_general | solution.py:799
  138.5 0.0 copy-start.2
  138.5 66.7 %collect.1 = bf16[2,16,8,2048]{3,2,1,0:T(8,128)(2,1)} custom-call(bf16[2,4,16,8,2048]{4,3,2,1,0:T(8,128)(2,1)} %bitcast.27), custom_call_target="tpu_custom_call" | custom-call | tf_op jit(solution)/shard_map/collect/pallas_call | solution.py:242
  205.2 0.0 copy-start.1
  205.2 0.0 copy-done.2
  205.2 1.6 fusion.10
  206.8 0.0 copy-done.1
  206.9 0.0 copy-start.3
  206.9 0.3 convolution_add_fusion
  207.2 0.8 dynamic-slice_bitcast_fusion
  208.0 2.7 %collective-permute-start = (f32[64,2048]{1,0:T(8,128)}, f32[64,2048]{1,0:T(8,128)}, u32[]{:S(2)}, u32[]{:S(2)}) collective-permute-start(f32[64,2048]{1,0:T(8,128)} %dynamic-slice_bitcast_fusion), channel_id=1, source_target_pairs={{0,4},{4,0},{1,5},{5,1},{2,6},{6,2},{3,7},{7,3},{8,12},{12,8},{9,1... | collective-permute-start | bytes 1572872 | tf_op jit(solution)/shard_map/ppermute | solution.py:813
  210.7 1.9 collective-permute-done
  212.6 0.0 copy-done.3
  212.6 1.8 fusion.7
Async XLA Ops:
  0.0 131.1 %copy-start = (bf16[2,256,2048]{2,1,0:T(8,128)(2,1)S(1)}, bf16[2,256,2048]{2,1,0:T(8,128)(2,1)}, u32[]{:S(2)}) copy-start(bf16[2,256,2048]{2,1,0:T(8,128)(2,1)} %param.36) | copy-start | bytes 6291460
  138.5 66.8 %copy-start.2 = (f32[128,256]{1,0:T(8,128)S(1)}, f32[128,256]{1,0:T(8,128)}, u32[]{:S(2)}) copy-start(f32[128,256]{1,0:T(8,128)} %get-tuple-element.9) | copy-start | bytes 393220
  205.2 1.6 copy-start.1
  206.9 5.7 %copy-start.3 = (bf16[64,2048]{1,0:T(8,128)(2,1)S(1)}, bf16[64,2048]{1,0:T(8,128)(2,1)}, u32[]{:S(2)}) copy-start(bf16[64,2048]{1,0:T(8,128)(2,1)} %get-tuple-element.8) | copy-start | bytes 786436
  208.0 4.6 %collective-permute-start = (f32[64,2048]{1,0:T(8,128)}, f32[64,2048]{1,0:T(8,128)}, u32[]{:S(2)}, u32[]{:S(2)}) collective-permute-start(f32[64,2048]{1,0:T(8,128)} %dynamic-slice_bitcast_fusion), channel_id=1, source_target_pairs={{0,4},{4,0},{1,5},{5,1},{2,6},{6,2},{3,7},{7,3},{8,12},{12,8},{9,1... | collective-permute-start | bytes 1572872 | tf_op jit(solution)/shard_map/ppermute | solution.py:813

commit v3 on v2

--- a/solution.py
+++ b/solution.py
@@ -22,7 +22,7 @@
 
 
 def greet(nz, nx):
-    z, x = lax.axis_index("sp_0"), lax.axis_index("tp")
+    z, c, x = lax.axis_index("sp_0"), lax.axis_index("sp_1"), lax.axis_index("tp")
     barrier = pltpu.get_barrier_semaphore()
 
     def signal(k, carry):
@@ -32,151 +32,150 @@
     lax.fori_loop(1, nz, signal, 0)
     pl.semaphore_signal(barrier, inc=1, device_id={"tp": lax.rem(x + 1, nx)})
     pl.semaphore_signal(barrier, inc=1, device_id={"tp": lax.rem(x + nx - 1, nx)})
-    pl.semaphore_wait(barrier, nz + 1)
-
-
-def dispatch_kernel(nz, nx, src, dst, zs, zr, xs, xr, fs, fr, here):
-    z, x = lax.axis_index("sp_0"), lax.axis_index("tp")
+    pl.semaphore_signal(barrier, inc=1, device_id={"sp_1": 1 - c})
+    pl.semaphore_wait(barrier, nz + 2)
+
+
+def experts_kernel(
+    nz,
+    nx,
+    src,
+    gates_hbm,
+    ups_hbm,
+    downs_hbm,
+    middle_ref,
+    weight_ref,
+    out_ref,
+    arrived,
+    part,
+    far,
+    near,
+    both,
+    mine,
+    total,
+    answers,
+    gates,
+    ups,
+    downs,
+    given,
+    taken,
+    load_sem,
+    here,
+    zs,
+    zr,
+    xs,
+    xr,
+    os_,
+    or_,
+    fs,
+    fr,
+    ns,
+    nr,
+    bs,
+    br,
+    ts,
+    tr,
+    ps,
+    pr,
+):
+    z, c, x = lax.axis_index("sp_0"), lax.axis_index("sp_1"), lax.axis_index("tp")
     xp, xm = lax.rem(x + 1, nx), lax.rem(x + nx - 1, nx)
     x2 = lax.rem(x + 2, nx)
+    local_experts, _, rows, width = src.shape
+    f32, bf16 = jnp.float32, jnp.bfloat16
+    loads = [
+        pltpu.make_async_copy(a, b, load_sem.at[n])
+        for n, (a, b) in enumerate(((gates_hbm, gates), (ups_hbm, ups), (downs_hbm, downs)))
+    ]
+    for load in loads:
+        load.start()
     greet(nz, nx)
 
-    def along_z(i):
-        to = lax.rem(z + hop(i) + nz, nz)
-        return pltpu.make_async_remote_copy(
-            src.at[:, to], dst.at[:, x, z], zs.at[i], zr.at[i], device_id={"sp_0": to}
-        )
+    def goal(i):
+        return lax.rem(z + hop(i) + nz, nz)
 
     def origin(i):
         return lax.rem(z - hop(i) + nz, nz)
 
+    def ahead(i):
+        return jnp.where(i % 2 == 0, xp, xm)
+
+    def behind(i):
+        return jnp.where(i % 2 == 0, xm, xp)
+
+    def remote(a, b, sent, got, **to):
+        return pltpu.make_async_remote_copy(a, b, sent, got, device_id=to)
+
+    def along_z(i):
+        return remote(src.at[:, goal(i)], arrived.at[i, :, x], zs.at[i], zr.at[i], sp_0=goal(i))
+
     def along_x(i, way):
-        chunk = dst.at[:, x, origin(i)]
+        chunk = arrived.at[i, :, x]
         to = xp if way == 0 else xm
-        return pltpu.make_async_remote_copy(
-            chunk, chunk, xs.at[way, i], xr.at[way, i], device_id={"tp": to}
-        )
-
-    def further(i):
-        way = i % 2
-        chunk = dst.at[:, jnp.where(way == 0, xm, xp), origin(i)]
-        to = jnp.where(way == 0, xp, xm)
-        return pltpu.make_async_remote_copy(
-            chunk, chunk, fs.at[i], fr.at[i], device_id={"tp": to}
-        )
-
-    def arrived_x(i, way):
-        chunk = dst.at[:, jnp.where(way == 0, xm, xp), origin(i)]
-        return pltpu.make_async_remote_copy(
-            chunk, chunk, xs.at[way, i], xr.at[way, i], device_id={"tp": xp}
-        )
-
-    def arrived_far(i):
-        chunk = dst.at[:, x2, origin(i)]
-        return pltpu.make_async_remote_copy(
-            chunk, chunk, fs.at[i], fr.at[i], device_id={"tp": xp}
-        )
+        return remote(chunk, chunk, xs.at[way, i], xr.at[way, i], tp=to)
+
+    def from_x(i, way):
+        chunk = arrived.at[i, :, jnp.where(way == 0, xm, xp)]
+        return remote(chunk, chunk, xs.at[way, i], xr.at[way, i], tp=xp)
+
+    def onward(i):
+        chunk = arrived.at[i, :, behind(i)]
+        return remote(chunk, chunk, os_.at[i], or_.at[i], tp=ahead(i))
+
+    def from_far(i):
+        chunk = arrived.at[i, :, x2]
+        return remote(chunk, chunk, os_.at[i], or_.at[i], tp=xp)
+
+    def send_far(i):
+        return remote(part.at[i, :, x2], far.at[i], fs.at[i], fr.at[i], tp=ahead(i))
+
+    def send_near(i):
+        return remote(part.at[i, :, behind(i)], near.at[i], ns.at[i], nr.at[i], tp=behind(i))
+
+    def send_both(i):
+        return remote(mine.at[i], both.at[i], bs.at[i], br.at[i], tp=ahead(i))
+
+    def send_back(i):
+        return remote(total.at[i], answers.at[:, z], ts.at[i], tr.at[i], sp_0=origin(i))
 
     def send_z(i, carry):
         along_z(i).start()
         return carry
 
     lax.fori_loop(1, nz, send_z, 0)
-    own = pltpu.make_async_copy(src.at[:, z], dst.at[:, x, z], here)
+    own = pltpu.make_async_copy(src.at[:, z], arrived.at[0, :, x], here.at[0])
     own.start()
     own.wait()
-    along_x(0, 0).start()
-    along_x(0, 1).start()
-
-    def spread(i, carry):
-        pltpu.make_async_remote_copy(
-            src.at[:, z], dst.at[:, x, origin(i)], zs.at[i], zr.at[i], device_id={"tp": xp}
-        ).wait_recv()
+
+    def spread(i):
         along_x(i, 0).start()
         along_x(i, 1).start()
-        arrived_x(i - 1, (i - 1) % 2).wait_recv()
-        further(i - 1).start()
-        return carry
-
-    lax.fori_loop(1, nz, spread, 0)
-    arrived_x(nz - 1, (nz - 1) % 2).wait_recv()
-    further(nz - 1).start()
-
-    def finish(i, carry):
-        arrived_x(i, (i + 1) % 2).wait_recv()
-        arrived_far(i).wait_recv()
-        along_x(i, 0).wait_send()
-        along_x(i, 1).wait_send()
-        further(i).wait_send()
-        return carry
-
-    lax.fori_loop(0, nz, finish, 0)
-
-    def sent(i, carry):
-        along_z(i).wait_send()
-        return carry
-
-    lax.fori_loop(1, nz, sent, 0)
-
-
-def dispatch(outgoing, nz, nx):
-    experts, _, rows, width = outgoing.shape
-    return pl.pallas_call(
-        functools.partial(dispatch_kernel, nz, nx),
-        out_shape=jax.ShapeDtypeStruct((experts, nx, nz, rows, width), outgoing.dtype),
-        in_specs=[pl.BlockSpec(memory_space=pltpu.VMEM)],
-        out_specs=pl.BlockSpec(memory_space=pltpu.VMEM),
-        scratch_shapes=[
-            pltpu.SemaphoreType.DMA((nz,)),
-            pltpu.SemaphoreType.DMA((nz,)),
-            pltpu.SemaphoreType.DMA((2, nz)),
-            pltpu.SemaphoreType.DMA((2, nz)),
-            pltpu.SemaphoreType.DMA((nz,)),
-            pltpu.SemaphoreType.DMA((nz,)),
-            pltpu.SemaphoreType.DMA,
-        ],
-        compiler_params=pltpu.CompilerParams(collective_id=1, has_side_effects=True),
-        name="dispatch",
-    )(outgoing)
-
-
-def collect_kernel(nz, nx, part, out, far, near, both, mine, total, fs, fr, ns, nr, bs, br, zs, zr, here):
-    z, x = lax.axis_index("sp_0"), lax.axis_index("tp")
-    xp, xm = lax.rem(x + 1, nx), lax.rem(x + nx - 1, nx)
-    x2 = lax.rem(x + 2, nx)
-    greet(nz, nx)
-
-    def step_of(s):
-        return nz - 1 - s
-
-    def goal(i):
-        return lax.rem(z + hop(i) + nz, nz)
-
-    def ahead(i):
-        return jnp.where(i % 2 == 0, xp, xm)
-
-    def behind(i):
-        return jnp.where(i % 2 == 0, xm, xp)
-
-    def send_far(i):
-        return pltpu.make_async_remote_copy(
-            part.at[:, x2, goal(i)], far.at[i], fs.at[i], fr.at[i], device_id={"tp": ahead(i)}
-        )
-
-    def send_near(i):
-        return pltpu.make_async_remote_copy(
-            part.at[:, behind(i), goal(i)], near.at[i], ns.at[i], nr.at[i], device_id={"tp": behind(i)}
-        )
-
-    def send_both(i):
-        return pltpu.make_async_remote_copy(
-            mine.at[i], both.at[i], bs.at[i], br.at[i], device_id={"tp": ahead(i)}
-        )
-
-    def send_z(i):
-        return pltpu.make_async_remote_copy(
-            total.at[i], out.at[:, z], zs.at[i], zr.at[i], device_id={"sp_0": goal(i)}
-        )
+
+    def pass_on(i):
+        from_x(i, i % 2).wait_recv()
+        onward(i).start()
+
+    def complete(i):
+        from_x(i, (i + 1) % 2).wait_recv()
+        from_far(i).wait_recv()
+
+    def multiply(i):
+        for e in range(local_experts):
+            tokens = jnp.concatenate(
+                [
+                    arrived[i + k, e].astype(f32).reshape(nx * rows, width).astype(bf16)
+                    for k in range(2)
+                ],
+                axis=0,
+            )
+            gate = jnp.dot(tokens, gates[e], preferred_element_type=f32)
+            up = jnp.dot(tokens, ups[e], preferred_element_type=f32)
+            hidden = (silu(gate) * up).astype(bf16)
+            result = jnp.dot(hidden, downs[e], preferred_element_type=f32)
+            for k in range(2):
+                part[i + k, e] = (
+                    result[k * nx * rows : (k + 1) * nx * rows].reshape(nx, rows, width).astype(bf16)
+                )
 
     def first(i):
         send_far(i).start()
@@ -184,72 +183,143 @@
 
     def second(i):
         send_far(i).wait_recv()
-        mine[i] = (
-            part[:, ahead(i), goal(i)].astype(jnp.float32) + far[i].astype(jnp.float32)
-        ).astype(mine.dtype)
+        mine[i] = (part[i, :, ahead(i)].astype(f32) + far[i].astype(f32)).astype(bf16)
         send_both(i).start()
 
     def third(i):
         send_near(i).wait_recv()
         send_both(i).wait_recv()
         total[i] = (
-            part[:, x, goal(i)].astype(jnp.float32)
-            + near[i].astype(jnp.float32)
-            + both[i].astype(jnp.float32)
-        ).astype(total.dtype)
-
-    first(step_of(0))
-    first(step_of(1))
-    second(step_of(0))
-
-    def turn(s, carry):
-        first(step_of(s))
-        second(step_of(s - 1))
-        third(step_of(s - 2))
-        send_z(step_of(s - 2)).start()
+            part[i, :, x].astype(f32) + near[i].astype(f32) + both[i].astype(f32)
+        ).astype(bf16)
+
+    pairs = nz // 2
+
+    def turn(p, carry):
+        i = 2 * p
+
+        @pl.when(p == 0)
+        def _():
+            spread(0)
+
+        @pl.when((p > 0) & (p < pairs))
+        def _():
+            remote(src.at[:, z], arrived.at[i, :, x], zs.at[i], zr.at[i], tp=xp).wait_recv()
+            spread(i)
+
+        @pl.when((p > 0) & (p <= pairs))
+        def _():
+            pass_on(i - 1)
+
+        @pl.when(p < pairs)
+        def _():
+            remote(src.at[:, z], arrived.at[i + 1, :, x], zs.at[i + 1], zr.at[i + 1], tp=xp).wait_recv()
+            spread(i + 1)
+            pass_on(i)
+
+        @pl.when(p == 1)
+        def _():
+            for load in loads:
+                load.wait()
+
+        @pl.when((p > 0) & (p <= pairs))
+        def _():
+            complete(i - 2)
+            complete(i - 1)
+            multiply(i - 2)
+            first(i - 2)
+            first(i - 1)
+
+        @pl.when((p > 1) & (p <= pairs + 1))
+        def _():
+            second(i - 4)
+            second(i - 3)
+
+        @pl.when(p > 2)
+        def _():
+            third(i - 6)
+            third(i - 5)
+
+            @pl.when(p > 3)
+            def _():
+                send_back(i - 6).start()
+
+            send_back(i - 5).start()
+
         return carry
 
-    lax.fori_loop(2, nz, turn, 0)
-    second(step_of(nz - 1))
-    third(step_of(nz - 2))
-    send_z(step_of(nz - 2)).start()
-    third(step_of(nz - 1))
-    own = pltpu.make_async_copy(total.at[0], out.at[:, z], here)
-    own.start()
-    own.wait()
-
-    def finish(i, carry):
+    lax.fori_loop(0, pairs + 3, turn, 0)
+    own_back = pltpu.make_async_copy(total.at[0], answers.at[:, z], here.at[1])
+    own_back.start()
+    own_back.wait()
+
+    def sent(i, carry):
+        along_x(i, 0).wait_send()
+        along_x(i, 1).wait_send()
+        onward(i).wait_send()
         send_far(i).wait_send()
         send_near(i).wait_send()
         send_both(i).wait_send()
         return carry
 
-    lax.fori_loop(0, nz, finish, 0)
-
-    def sent(i, carry):
-        send_z(i).wait_send()
-        pltpu.make_async_remote_copy(
-            total.at[i], out.at[:, lax.rem(z - hop(i) + nz, nz)], zs.at[i], zr.at[i], device_id={"tp": xp}
-        ).wait_recv()
+    lax.fori_loop(0, nz, sent, 0)
+
+    def returned(i, carry):
+        along_z(i).wait_send()
+        send_back(i).wait_send()
+        remote(total.at[i], answers.at[:, goal(i)], ts.at[i], tr.at[i], tp=xp).wait_recv()
         return carry
 
-    lax.fori_loop(1, nz, sent, 0)
-
-
-def collect(part, nz, nx):
-    experts, _, _, rows, width = part.shape
-    slots = pltpu.VMEM((nz, experts, rows, width), part.dtype)
+    lax.fori_loop(1, nz, returned, 0)
+
+    count = out_ref.shape[0]
+    slots = local_experts * nz * rows
+    known = answers[...].astype(f32).reshape(slots, width).astype(bf16)
+
+    def shared(start):
+        weight = weight_ref[pl.ds(pl.multiple_of(start * count, count), count), :]
+        high = weight.astype(bf16)
+        low = (weight - high.astype(f32)).astype(bf16)
+        return jnp.dot(high, known, preferred_element_type=f32) + jnp.dot(
+            low, known, preferred_element_type=f32
+        )
+
+    given[...] = shared(1 - c)
+    swap = remote(given, taken, ps, pr, sp_1=1 - c)
+    swap.start()
+    kept = middle_ref[...].astype(f32) + shared(c)
+    swap.wait()
+    out_ref[...] = (kept + taken[...]).astype(bf16)
+
+
+def routed(outgoing, gates, ups, downs, middle, weight, nz, nx):
+    experts, _, rows, width = outgoing.shape
+    bf16 = jnp.bfloat16
+    slots = pltpu.VMEM((nz, experts, rows, width), bf16)
+    wide = pltpu.VMEM((nz, experts, nx, rows, width), bf16)
+    count = middle.shape[0]
+    vmem = pl.BlockSpec(memory_space=pltpu.VMEM)
+    anywhere = pl.BlockSpec(memory_space=pl.ANY)
+    line = pltpu.SemaphoreType.DMA((nz,))
     return pl.pallas_call(
-        functools.partial(collect_kernel, nz, nx),
-        out_shape=jax.ShapeDtypeStruct((experts, nz, rows, width), part.dtype),
-        in_specs=[pl.BlockSpec(memory_space=pltpu.VMEM)],
-        out_specs=pl.BlockSpec(memory_space=pltpu.VMEM),
-        scratch_shapes=[slots] * 5
-        + [pltpu.SemaphoreType.DMA((nz,))] * 8
-        + [pltpu.SemaphoreType.DMA],
-        compiler_params=pltpu.CompilerParams(collective_id=2, has_side_effects=True),
-        name="collect",
-    )(part)
+        functools.partial(experts_kernel, nz, nx),
+        out_shape=jax.ShapeDtypeStruct((count, width), bf16),
+        in_specs=[vmem, anywhere, anywhere, anywhere, vmem, vmem],
+        out_specs=vmem,
+        scratch_shapes=[wide, wide, slots, slots, slots, slots, slots]
+        + [pltpu.VMEM((experts, nz, rows, width), bf16)]
+        + [pltpu.VMEM(w.shape, bf16) for w in (gates, ups, downs)]
+        + [pltpu.VMEM((count, width), jnp.float32)] * 2
+        + [pltpu.SemaphoreType.DMA((3,)), pltpu.SemaphoreType.DMA((2,))]
+        + [line, line]
+        + [pltpu.SemaphoreType.DMA((2, nz))] * 2
+        + [line] * 10
+        + [pltpu.SemaphoreType.DMA] * 2,
+        compiler_params=pltpu.CompilerParams(
+            collective_id=1, has_side_effects=True, vmem_limit_bytes=60 << 20
+        ),
+        name="experts",
+    )(outgoing, gates, ups, downs, middle, weight)
 
 
 QUAD = 4
@@ -333,7 +403,9 @@
     raw_ref,
     extra_ref,
     rate_ref,
-    taps_ref,
+    taps_x_ref,
+    taps_k_ref,
+    taps_q_ref,
     gain_ref,
     blend_hbm,
     carry_ref,
@@ -359,6 +431,7 @@
     facts,
     rows,
     blend,
+    turned,
     blend_sem,
     halo_s,
     halo_r,
@@ -374,7 +447,7 @@
     z, c, x = lax.axis_index("sp_0"), lax.axis_index("sp_1"), lax.axis_index("tp")
     length, width_x = xs_ref.shape
     state_width = keys_ref.shape[1]
-    heads = raw_ref.shape[1]
+    heads = raw_ref.shape[0]
     head_dim = width_x // heads
     half_heads = heads // 2
     half_rows = width_x // 2
@@ -385,18 +458,53 @@
     load = pltpu.make_async_copy(blend_hbm, blend, blend_sem)
     load.start()
 
-    count, picks = ids_ref.shape[0] // nx, ids_ref.shape[1]
+    stride_row = jnp.maximum(raw_ref[...], 0.0) + jnp.log1p(jnp.exp(-jnp.abs(raw_ref[...])))
+    diagonal = lax.broadcasted_iota(jnp.int32, (heads, heads), 0) == lax.broadcasted_iota(
+        jnp.int32, (heads, heads), 1
+    )
+    rate = jnp.sum(
+        jnp.where(diagonal, jnp.broadcast_to(rate_ref[...], (heads, heads)), 0.0),
+        axis=1,
+        keepdims=True,
+    )
+    log_row = extra_ref[...] - rate * stride_row
+    t_axis = lax.broadcasted_iota(jnp.int32, (length, length), 0)
+    s_axis = lax.broadcasted_iota(jnp.int32, (length, length), 1)
+    causal = t_axis >= s_axis
+    running_row = exact_dot(
+        jnp.concatenate([log_row, jnp.zeros_like(log_row)], axis=0), (t_axis <= s_axis).astype(f32)
+    )
+    picks = ids_ref.shape[0]
+    count = ids_ref.shape[1] // nx
+    lanes = 128
+    stacked = jnp.concatenate(
+        [
+            running_row[:heads],
+            stride_row,
+            ids_ref[...].astype(f32),
+            jnp.zeros((lanes - 2 * heads - picks, length), f32),
+        ],
+        axis=0,
+    )
+    turned[...] = stacked.T
+    running = turned[:, :heads]
+    stride = turned[:, heads : 2 * heads]
+    final = running[length - 1 : length, :]
+    lifted = jnp.exp(affinity_ref[...])
+    share_row = chance_ref[...] * lifted / jnp.sum(lifted, axis=0, keepdims=True)
+    share_row = jnp.concatenate([share_row, jnp.zeros((lanes - picks, count), f32)], axis=0)
+    share_row = jnp.concatenate([share_row, jnp.zeros((lanes, lanes - count), f32)], axis=1)
+    shares = share_row.T[:count]
     local_experts = outgoing_ref.shape[0]
     experts = nz * 2 * local_experts
-    ids = ids_ref[pl.ds(pl.multiple_of(x * count, count), count), :]
+    ids = turned[pl.ds(pl.multiple_of(x * count, count), count), :]
+    ids = ids[:, 2 * heads : 2 * heads + picks].astype(jnp.int32)
     expert_axis = lax.broadcasted_iota(jnp.int32, (count, experts), 1)
     member = [(ids[:, k : k + 1] == expert_axis).astype(f32) for k in range(picks)]
     row_axis = lax.broadcasted_iota(jnp.int32, (count, count), 0)
     column_axis = lax.broadcasted_iota(jnp.int32, (count, count), 1)
     earlier = (row_axis > column_axis).astype(bf16)
     before = jnp.dot(earlier, sum(member).astype(bf16), preferred_element_type=f32)
-    lifted = jnp.exp(affinity_ref[...])
-    shares = chance_ref[...] * lifted / jnp.sum(lifted, axis=1, keepdims=True)
     lane = lax.broadcasted_iota(jnp.int32, (count, facts.shape[2]), 1)
     noted = jnp.zeros((count, facts.shape[2]), f32)
     for k in range(picks):
@@ -436,19 +544,6 @@
     )
     facts_copy.start()
 
-    stride = jnp.maximum(raw_ref[...], 0.0) + jnp.log1p(jnp.exp(-jnp.abs(raw_ref[...])))
-    log_decay = extra_ref[...] - rate_ref[...] * stride
-    lane = lax.broadcasted_iota(jnp.int32, (length, 128), 1)
-    padded = jnp.zeros((length, 128), f32)
-    for h in range(heads):
-        padded = jnp.where(lane == h, log_decay[:, h : h + 1], padded)
-    t_axis = lax.broadcasted_iota(jnp.int32, (length, length), 0)
-    s_axis = lax.broadcasted_iota(jnp.int32, (length, length), 1)
-    causal = t_axis >= s_axis
-    running = exact_dot(causal.astype(f32), padded)
-    running_row = running.T
-    final = running[length - 1 : length, :]
-
     start = 0
     for ref in (xs_ref, keys_ref, queries_ref):
         joined[rim:, start : start + ref.shape[1]] = ref[...].astype(f32)
@@ -456,11 +551,12 @@
     for edge in edges:
         edge.wait_recv()
     joined[:rim, :] = jnp.where(z + c > 0, halo[...].astype(f32), 0.0)
-    kernel_len = taps_ref.shape[0]
-    convolved = taps_ref[0:1, :] * joined[rim - kernel_len + 1 : rim - kernel_len + 1 + length, :]
+    taps = jnp.concatenate([taps_x_ref[...], taps_k_ref[...], taps_q_ref[...]], axis=1)
+    kernel_len = taps.shape[0]
+    convolved = taps[0:1, :] * joined[rim - kernel_len + 1 : rim - kernel_len + 1 + length, :]
     for tap in range(1, kernel_len):
         first = rim - kernel_len + 1 + tap
-        convolved = convolved + taps_ref[tap : tap + 1, :] * joined[first : first + length, :]
+        convolved = convolved + taps[tap : tap + 1, :] * joined[first : first + length, :]
     convolved = silu(convolved)
     inputs_x = convolved[:, :width_x]
     keys_b = convolved[:, width_x : width_x + state_width].astype(bf16)
@@ -680,7 +776,7 @@
 
 def front(nz, nx, local_experts, capacity, *arrays):
     xs, _, keys, queries, raw = arrays[:5]
-    blend, carry = arrays[9:11]
+    blend, carry = arrays[11:13]
     count, width = carry.shape
     slots = local_experts * nz * 2 * capacity
     channels = xs.shape[1]
@@ -697,7 +793,7 @@
             jax.ShapeDtypeStruct((count, width), bf16),
             jax.ShapeDtypeStruct((2 * count, slots), jnp.float32),
         ),
-        in_specs=[vmem] * 9 + [pl.BlockSpec(memory_space=pl.ANY)] + [vmem] * 5,
+        in_specs=[vmem] * 11 + [pl.BlockSpec(memory_space=pl.ANY)] + [vmem] * 5,
         out_specs=(vmem, vmem, vmem),
         scratch_shapes=[
             pltpu.VMEM((rim, total), bf16),
@@ -715,6 +811,7 @@
             pltpu.VMEM((2, count, 128), jnp.float32),
             pltpu.VMEM((2, count, width), bf16),
             pltpu.VMEM(blend.shape, bf16),
+            pltpu.VMEM((xs.shape[0], 128), jnp.float32),
             pltpu.SemaphoreType.DMA,
             pltpu.SemaphoreType.DMA((3,)),
             pltpu.SemaphoreType.DMA((3,)),
@@ -755,16 +852,11 @@
     cluster_chance,
 ):
     nz, cores, nx = lax.axis_size("sp_0"), lax.axis_size("sp_1"), lax.axis_size("tp")
-    core = lax.axis_index("sp_1")
     row_count, model_width = carryover_vector.shape
     local_experts = specialist_gating_matrices.shape[0]
     experts = nz * cores * local_experts
     picks = assigned_specialist_ids.shape[1]
     capacity = 2 * row_count * picks // experts
-    per_core = cores * capacity
-    taps = jnp.concatenate(
-        [channel_source_kernel, entering_basis_kernel, readout_basis_kernel], axis=1
-    )
     outgoing, middle, weight_of = front(
         nz,
         nx,
@@ -774,44 +866,30 @@
         final_modulation_vector,
         entering_basis_matrix,
         readout_basis_matrix,
-        raw_stride_amount,
-        extra_log_attenuation,
+        raw_stride_amount.T,
+        extra_log_attenuation.T,
         channel_fading_rate[None, :],
-        taps,
+        channel_source_kernel,
+        entering_basis_kernel,
+        readout_basis_kernel,
         modulated_rescaling_vector[None, :],
         blender_final_matrix,
         carryover_vector,
         specialist_rescaling_vector[None, :],
-        assigned_specialist_ids,
-        specialist_choice_affinity,
-        cluster_chance[:, None],
-    )
-    middle_wide = middle.astype(jnp.float32)
-    slot_count = weight_of.shape[1]
-    arrived = dispatch(outgoing, nz, nx).reshape(local_experts, -1, model_width)
-    gate_value = jnp.einsum(
-        "lrd,ldf->lrf", arrived, specialist_gating_matrices, preferred_element_type=jnp.float32
-    )
-    up_value = jnp.einsum(
-        "lrd,ldf->lrf", arrived, widening_matrices, preferred_element_type=jnp.float32
-    )
-    hidden = (jax.nn.silu(gate_value) * up_value).astype(jnp.bfloat16)
-    partial_value = jnp.einsum(
-        "lrf,lfd->lrd", hidden, contracting_matrices, preferred_element_type=jnp.float32
-    ).astype(jnp.bfloat16)
-    answers = collect(
-        partial_value.reshape(local_experts, nx, nz, per_core, model_width), nz, nx
-    ).reshape(slot_count, model_width)
-    weight_high = weight_of.astype(jnp.bfloat16)
-    weight_low = (weight_of - weight_high.astype(jnp.float32)).astype(jnp.bfloat16)
-    gathered = jnp.dot(weight_high, answers, preferred_element_type=jnp.float32) + jnp.dot(
-        weight_low, answers, preferred_element_type=jnp.float32
-    )
-    gathered = gathered.reshape(cores, row_count, model_width)
-    kept = lax.dynamic_index_in_dim(gathered, core, 0, keepdims=False)
-    given = lax.dynamic_index_in_dim(gathered, cores - 1 - core, 0, keepdims=False)
-    taken = lax.ppermute(given, "sp_1", [(0, 1), (1, 0)])
-    return (middle_wide + (kept + taken)).astype(jnp.bfloat16)
+        assigned_specialist_ids.T,
+        specialist_choice_affinity.T,
+        cluster_chance[None, :],
+    )
+    return routed(
+        outgoing,
+        specialist_gating_matrices,
+        widening_matrices,
+        contracting_matrices,
+        middle,
+        weight_of,
+        nz,
+        nx,
+    )
 
 
 def solution(mesh):

time: 215 us -> 181 us (0.84)
  matrix products: 13.3 us -> 0 us
  local copies, waits for them, and re-layouts: 8.15 us -> 1.67 us
  Pallas kernels: 185 us -> 179 us
  other arithmetic: 3.13 us -> 0 us
  starting transfers between devices: 2.69 us -> 0 us
    dot_general x4 -> x0, matrix products: 13.3 us -> none  [the longest x1 7.31 us: per_device(): jnp.einsum('lrf,lfd->lrd', hidden, contracting_matrices, preferred_elemen...]
    pallas_call x2 -> x1, Pallas kernels: 140 us -> 133 us  [routed(): pl.pallas_call(functools.partial(experts_kernel, nz, nx), out_shape=jax.S...]
    unnamed x12 -> x1, local copies, waits for them, and re-layouts: 5.96 us -> 1.67 us
    ppermute x1 -> x0, starting transfers between devices: 2.69 us -> none  [per_device(): taken = lax.ppermute(given, 'sp_1', [(0, 1), (1, 0)])]
  transfers between devices with their start and end apart: 1 -> 0, of which waited for: 1 -> 0; matrix products, arithmetic and copies ran while one was open for 0% -> 0% of each run, Pallas kernels for 0% -> 0%
where the time goes in v3:
time: 181 us
  Pallas kernels  179 us (99%)
    pallas_call x1, Pallas kernels, routed(): pl.pallas_call(functools.partial(experts_kernel, nz, nx), out_shape=jax.S...  133 us
    pallas_call x1, Pallas kernels, front(): pl.pallas_call(functools.partial(front_kernel, nz, nx, capacity), out_sha...  45.7 us

profile of v3, /device:TPU:33, one launch (start us, length us, event | category | flops | bytes accessed | tf_op | source)
XLA Modules:
  0.0 180.7 jit_solution(9632494462312271795)
XLA Ops:
  0.0 45.7 %front.1 = (bf16[2,16,8,2048]{3,2,1,0:T(8,128)(2,1)}, bf16[64,2048]{1,0:T(8,128)(2,1)}, f32[128,256]{1,0:T(8,128)}) custom-call(bf16[256,256]{1,0:T(8,128)(2,1)} %xs_ref.1, bf16[256,256]{1,0:T(8,128)(2,1)} %gate_ref.1, bf16[256,128]{1,0:T(8,128)(2,1)} %keys_ref.1, bf16[256,128]{1,0:T(8,128)(2,1)} %queries_ref.1, f32[4,256]{1,0:T(4,128)} %bitcast.9, ...), custom_call_target="tpu_custom_call" | custom-call | tf_op jit(solution)/shard_map/front/pallas_call | solution.py:789
  45.7 133.4 %experts.1 = bf16[64,2048]{1,0:T(8,128)(2,1)} custom-call(bf16[2,16,8,2048]{3,2,1,0:T(8,128)(2,1)} %get-tuple-element.8.src, bf16[2,2048,256]{2,1,0:T(8,128)(2,1)} %gates_hbm.1, bf16[2,2048,256]{2,1,0:T(8,128)(2,1)} %ups_hbm.1, bf16[2,256,2048]{2,1,0:T(8,128)(2,1)} %downs_hbm.1, bf16[64,2048]{1,0:T(8,128)(2,1)} %get-tuple-element.9.middle_ref, ...), custom_call_target="tpu_custom_call" | custom-call | tf_op jit(solution)/shard_map/experts/pallas_call | solution.py:304
  179.1 1.7 copy.22

commit v4 on v3

--- a/solution.py
+++ b/solution.py
@@ -16,7 +16,11 @@
 EPS = 1e-06
 
 
-def hop(step):
+NEAR = 4
+
+
+def hop(step, nz):
+    step = jnp.where(step > NEAR, nz + NEAR - step, step)
     half = (step + 1) // 2
     return jnp.where(step % 2 == 1, half, -half)
 
@@ -92,10 +96,10 @@
     greet(nz, nx)
 
     def goal(i):
-        return lax.rem(z + hop(i) + nz, nz)
+        return lax.rem(z + hop(i, nz) + nz, nz)
 
     def origin(i):
-        return lax.rem(z - hop(i) + nz, nz)
+        return lax.rem(z - hop(i, nz) + nz, nz)
 
     def ahead(i):
         return jnp.where(i % 2 == 0, xp, xm)

time: 181 us -> 174 us (0.961)
  Pallas kernels: 179 us -> 171 us
    pallas_call x1, Pallas kernels: 133 us -> 125 us  [routed(): pl.pallas_call(functools.partial(experts_kernel, nz, nx), out_shape=jax.S...]
where the time goes in v4:
time: 174 us; the launch traced here: 173 us
  Pallas kernels  171 us (98%)
    pallas_call x1, Pallas kernels, routed(): pl.pallas_call(functools.partial(experts_kernel, nz, nx), out_shape=jax.S...  125 us
    pallas_call x1, Pallas kernels, front(): pl.pallas_call(functools.partial(front_kernel, nz, nx, capacity), out_sha...  45.7 us

profile of v4, /device:TPU:33, one launch (start us, length us, event | category | flops | bytes accessed | tf_op | source)
XLA Modules:
  0.0 172.8 jit_solution(13657257639652341275)
XLA Ops:
  0.0 45.7 %front.1 = (bf16[2,16,8,2048]{3,2,1,0:T(8,128)(2,1)}, bf16[64,2048]{1,0:T(8,128)(2,1)}, f32[128,256]{1,0:T(8,128)}) custom-call(bf16[256,256]{1,0:T(8,128)(2,1)} %xs_ref.1, bf16[256,256]{1,0:T(8,128)(2,1)} %gate_ref.1, bf16[256,128]{1,0:T(8,128)(2,1)} %keys_ref.1, bf16[256,128]{1,0:T(8,128)(2,1)} %queries_ref.1, f32[4,256]{1,0:T(4,128)} %bitcast.9, ...), custom_call_target="tpu_custom_call" | custom-call | tf_op jit(solution)/shard_map/front/pallas_call | solution.py:793
  45.7 125.5 %experts.1 = bf16[64,2048]{1,0:T(8,128)(2,1)} custom-call(bf16[2,16,8,2048]{3,2,1,0:T(8,128)(2,1)} %get-tuple-element.8.src, bf16[2,2048,256]{2,1,0:T(8,128)(2,1)} %gates_hbm.1, bf16[2,2048,256]{2,1,0:T(8,128)(2,1)} %ups_hbm.1, bf16[2,256,2048]{2,1,0:T(8,128)(2,1)} %downs_hbm.1, bf16[64,2048]{1,0:T(8,128)(2,1)} %get-tuple-element.9.middle_ref, ...), custom_call_target="tpu_custom_call" | custom-call | tf_op jit(solution)/shard_map/experts/pallas_call | solution.py:308
  171.2 1.7 copy.22

commit v5 on v4

--- a/solution.py
+++ b/solution.py
@@ -23,21 +23,6 @@
     step = jnp.where(step > NEAR, nz + NEAR - step, step)
     half = (step + 1) // 2
     return jnp.where(step % 2 == 1, half, -half)
-
-
-def greet(nz, nx):
-    z, c, x = lax.axis_index("sp_0"), lax.axis_index("sp_1"), lax.axis_index("tp")
-    barrier = pltpu.get_barrier_semaphore()
-
-    def signal(k, carry):
-        pl.semaphore_signal(barrier, inc=1, device_id={"sp_0": lax.rem(z + k, nz)})
-        return carry
-
-    lax.fori_loop(1, nz, signal, 0)
-    pl.semaphore_signal(barrier, inc=1, device_id={"tp": lax.rem(x + 1, nx)})
-    pl.semaphore_signal(barrier, inc=1, device_id={"tp": lax.rem(x + nx - 1, nx)})
-    pl.semaphore_signal(barrier, inc=1, device_id={"sp_1": 1 - c})
-    pl.semaphore_wait(barrier, nz + 2)
 
 
 def experts_kernel(
@@ -93,7 +78,6 @@
     ]
     for load in loads:
         load.start()
-    greet(nz, nx)
 
     def goal(i):
         return lax.rem(z + hop(i, nz) + nz, nz)
@@ -296,41 +280,11 @@
     out_ref[...] = (kept + taken[...]).astype(bf16)
 
 
-def routed(outgoing, gates, ups, downs, middle, weight, nz, nx):
-    experts, _, rows, width = outgoing.shape
-    bf16 = jnp.bfloat16
-    slots = pltpu.VMEM((nz, experts, rows, width), bf16)
-    wide = pltpu.VMEM((nz, experts, nx, rows, width), bf16)
-    count = middle.shape[0]
-    vmem = pl.BlockSpec(memory_space=pltpu.VMEM)
-    anywhere = pl.BlockSpec(memory_space=pl.ANY)
-    line = pltpu.SemaphoreType.DMA((nz,))
-    return pl.pallas_call(
-        functools.partial(experts_kernel, nz, nx),
-        out_shape=jax.ShapeDtypeStruct((count, width), bf16),
-        in_specs=[vmem, anywhere, anywhere, anywhere, vmem, vmem],
-        out_specs=vmem,
-        scratch_shapes=[wide, wide, slots, slots, slots, slots, slots]
-        + [pltpu.VMEM((experts, nz, rows, width), bf16)]
-        + [pltpu.VMEM(w.shape, bf16) for w in (gates, ups, downs)]
-        + [pltpu.VMEM((count, width), jnp.float32)] * 2
-        + [pltpu.SemaphoreType.DMA((3,)), pltpu.SemaphoreType.DMA((2,))]
-        + [line, line]
-        + [pltpu.SemaphoreType.DMA((2, nz))] * 2
-        + [line] * 10
-        + [pltpu.SemaphoreType.DMA] * 2,
-        compiler_params=pltpu.CompilerParams(
-            collective_id=1, has_side_effects=True, vmem_limit_bytes=60 << 20
-        ),
-        name="experts",
-    )(outgoing, gates, ups, downs, middle, weight)
-
-
 QUAD = 4
 TAIL = 16
 
 
-def greet_all(nz, nx):
+def announce(nz, nx):
     z, c, x = lax.axis_index("sp_0"), lax.axis_index("sp_1"), lax.axis_index("tp")
     barrier = pltpu.get_barrier_semaphore()
 
@@ -348,7 +302,6 @@
     pl.semaphore_signal(
         barrier, inc=1, device_id={"sp_0": lax.rem(z + nz - 1 + 2 * c, nz), "sp_1": 1 - c}
     )
-    pl.semaphore_wait(barrier, nz + nx)
 
 
 def silu(v):
@@ -459,6 +412,7 @@
     quads = nz // QUAD
     f32, bf16 = jnp.float32, jnp.bfloat16
     partner = {"sp_1": 1 - c}
+    announce(nz, nx)
     load = pltpu.make_async_copy(blend_hbm, blend, blend_sem)
     load.start()
 
@@ -524,7 +478,7 @@
         noted = jnp.where(lane == 2 * picks + k, shares[:, k : k + 1], noted)
     facts[c] = noted
 
-    greet_all(nz, nx)
+    pl.semaphore_wait(pltpu.get_barrier_semaphore(), nz + nx)
     rim = halo.shape[0]
     after = {"sp_0": lax.rem(z + c, nz), "sp_1": 1 - c}
     edges = []
@@ -778,58 +732,93 @@
         gated_send(k).wait_send()
 
 
-def front(nz, nx, local_experts, capacity, *arrays):
+FRONT_INPUTS = 17
+FRONT_SCRATCH = 27
+
+
+def layer_kernel(nz, nx, capacity, *refs):
+    inputs, refs = refs[:FRONT_INPUTS], refs[FRONT_INPUTS:]
+    weights, out_ref, refs = refs[:3], refs[3], refs[4:]
+    outgoing, middle, weight, refs = *refs[:3], refs[3:]
+    front_kernel(nz, nx, capacity, *inputs, outgoing, middle, weight, *refs[:FRONT_SCRATCH])
+    experts_kernel(nz, nx, outgoing, *weights, middle, weight, out_ref, *refs[FRONT_SCRATCH:])
+
+
+def layer(nz, nx, capacity, *arrays):
     xs, _, keys, queries, raw = arrays[:5]
     blend, carry = arrays[11:13]
+    weights = arrays[FRONT_INPUTS:]
+    experts = weights[0].shape[0]
     count, width = carry.shape
-    slots = local_experts * nz * 2 * capacity
-    channels = xs.shape[1]
-    total = channels + keys.shape[1] + queries.shape[1]
+    rows = 2 * capacity
+    channels, states = xs.shape[1], keys.shape[1]
+    total = channels + states + queries.shape[1]
     rim = 8
-    states = keys.shape[1]
-    bf16 = jnp.bfloat16
+    half = channels // 2
+    bf16, f32 = jnp.bfloat16, jnp.float32
     vmem = pl.BlockSpec(memory_space=pltpu.VMEM)
-    half = channels // 2
+    anywhere = pl.BlockSpec(memory_space=pl.ANY)
+    slots = pltpu.VMEM((nz, experts, rows, width), bf16)
+    wide = pltpu.VMEM((nz, experts, nx, rows, width), bf16)
+
+    def sems(*shape):
+        return pltpu.SemaphoreType.DMA(shape)
+
+    front_scratch = [
+        pltpu.VMEM((rim, total), bf16),
+        pltpu.VMEM((rim + xs.shape[0], total), f32),
+        pltpu.VMEM((channels + TAIL, states), bf16),
+        pltpu.VMEM((channels + TAIL, states), bf16),
+        pltpu.VMEM((half + TAIL, states), bf16),
+        pltpu.VMEM((QUAD, half + TAIL, states), bf16),
+        pltpu.VMEM((half + TAIL, states), bf16),
+        pltpu.VMEM((nz // QUAD, half + TAIL, states), bf16),
+        pltpu.VMEM((half, states), bf16),
+        pltpu.VMEM((half, states), bf16),
+        pltpu.VMEM((nx, count, channels), bf16),
+        pltpu.VMEM((nx, count, channels), bf16),
+        pltpu.VMEM((2, count, 128), f32),
+        pltpu.VMEM((2, count, width), bf16),
+        pltpu.VMEM(blend.shape, bf16),
+        pltpu.VMEM((xs.shape[0], 128), f32),
+        pltpu.SemaphoreType.DMA,
+        sems(3),
+        sems(3),
+        sems(4),
+        sems(4),
+        sems(QUAD),
+        sems(QUAD),
+        sems(nz // QUAD),
+        sems(nz // QUAD),
+        sems(nx),
+        sems(nx),
+    ]
+    experts_scratch = (
+        [wide, wide, slots, slots, slots, slots, slots]
+        + [pltpu.VMEM((experts, nz, rows, width), bf16)]
+        + [pltpu.VMEM(w.shape, bf16) for w in weights]
+        + [pltpu.VMEM((count, width), f32)] * 2
+        + [sems(3), sems(2), sems(nz), sems(nz), sems(2, nz), sems(2, nz)]
+        + [sems(nz)] * 10
+        + [pltpu.SemaphoreType.DMA] * 2
+    )
+    assert len(front_scratch) == FRONT_SCRATCH
     return pl.pallas_call(
-        functools.partial(front_kernel, nz, nx, capacity),
-        out_shape=(
-            jax.ShapeDtypeStruct((local_experts, nz, 2 * capacity, width), bf16),
-            jax.ShapeDtypeStruct((count, width), bf16),
-            jax.ShapeDtypeStruct((2 * count, slots), jnp.float32),
+        functools.partial(layer_kernel, nz, nx, capacity),
+        out_shape=jax.ShapeDtypeStruct((count, width), bf16),
+        in_specs=[vmem] * 11 + [anywhere] + [vmem] * 5 + [anywhere] * 3,
+        out_specs=vmem,
+        scratch_shapes=[
+            pltpu.VMEM((experts, nz, rows, width), bf16),
+            pltpu.VMEM((count, width), bf16),
+            pltpu.VMEM((2 * count, experts * nz * rows), f32),
+        ]
+        + front_scratch
+        + experts_scratch,
+        compiler_params=pltpu.CompilerParams(
+            collective_id=1, has_side_effects=True, vmem_limit_bytes=60 << 20
         ),
-        in_specs=[vmem] * 11 + [pl.BlockSpec(memory_space=pl.ANY)] + [vmem] * 5,
-        out_specs=(vmem, vmem, vmem),
-        scratch_shapes=[
-            pltpu.VMEM((rim, total), bf16),
-            pltpu.VMEM((rim + xs.shape[0], total), jnp.float32),
-            pltpu.VMEM((channels + TAIL, states), bf16),
-            pltpu.VMEM((channels + TAIL, states), bf16),
-            pltpu.VMEM((half + TAIL, states), bf16),
-            pltpu.VMEM((QUAD, half + TAIL, states), bf16),
-            pltpu.VMEM((half + TAIL, states), bf16),
-            pltpu.VMEM((nz // QUAD, half + TAIL, states), bf16),
-            pltpu.VMEM((half, states), bf16),
-            pltpu.VMEM((half, states), bf16),
-            pltpu.VMEM((nx, count, channels), bf16),
-            pltpu.VMEM((nx, count, channels), bf16),
-            pltpu.VMEM((2, count, 128), jnp.float32),
-            pltpu.VMEM((2, count, width), bf16),
-            pltpu.VMEM(blend.shape, bf16),
-            pltpu.VMEM((xs.shape[0], 128), jnp.float32),
-            pltpu.SemaphoreType.DMA,
-            pltpu.SemaphoreType.DMA((3,)),
-            pltpu.SemaphoreType.DMA((3,)),
-            pltpu.SemaphoreType.DMA((4,)),
-            pltpu.SemaphoreType.DMA((4,)),
-            pltpu.SemaphoreType.DMA((QUAD,)),
-            pltpu.SemaphoreType.DMA((QUAD,)),
-            pltpu.SemaphoreType.DMA((nz // QUAD,)),
-            pltpu.SemaphoreType.DMA((nz // QUAD,)),
-            pltpu.SemaphoreType.DMA((nx,)),
-            pltpu.SemaphoreType.DMA((nx,)),
-        ],
-        compiler_params=pltpu.CompilerParams(collective_id=3, has_side_effects=True),
-        name="front",
+        name="layer",
     )(*arrays)
 
 
@@ -856,15 +845,14 @@
     cluster_chance,
 ):
     nz, cores, nx = lax.axis_size("sp_0"), lax.axis_size("sp_1"), lax.axis_size("tp")
-    row_count, model_width = carryover_vector.shape
+    row_count = carryover_vector.shape[0]
     local_experts = specialist_gating_matrices.shape[0]
     experts = nz * cores * local_experts
     picks = assigned_specialist_ids.shape[1]
     capacity = 2 * row_count * picks // experts
-    outgoing, middle, weight_of = front(
+    return layer(
         nz,
         nx,
-        local_experts,
         capacity,
         channel_source_entries,
         final_modulation_vector,
@@ -883,16 +871,9 @@
         assigned_specialist_ids.T,
         specialist_choice_affinity.T,
         cluster_chance[None, :],
-    )
-    return routed(
-        outgoing,
         specialist_gating_matrices,
         widening_matrices,
         contracting_matrices,
-        middle,
-        weight_of,
-        nz,
-        nx,
     )
 
 

time: 174 us -> 166 us (0.954)
  Pallas kernels: 171 us -> 164 us
    pallas_call x2 -> x1, Pallas kernels: 171 us -> 164 us  [layer(): pl.pallas_call(functools.partial(layer_kernel, nz, nx, capacity), out_sha...]
where the time goes in v5:
time: 166 us
  Pallas kernels  164 us (99%)
  local copies, waits for them, and re-layouts  1.67 us (1%)
    pallas_call x1, Pallas kernels, layer(): pl.pallas_call(functools.partial(layer_kernel, nz, nx, capacity), out_sha...  164 us

profile of v5, /device:TPU:33, one launch (start us, length us, event | category | flops | bytes accessed | tf_op | source)
XLA Modules:
  0.0 165.6 jit_solution(6277421184301564285)
XLA Ops:
  0.0 164.0 %layer.1 = bf16[64,2048]{1,0:T(8,128)(2,1)} custom-call(bf16[256,256]{1,0:T(8,128)(2,1)} %refs_0_.1, bf16[256,256]{1,0:T(8,128)(2,1)} %refs_1_.1, bf16[256,128]{1,0:T(8,128)(2,1)} %refs_2_.1, bf16[256,128]{1,0:T(8,128)(2,1)} %refs_3_.1, f32[4,256]{1,0:T(4,128)} %bitcast.9, f32[4,256]{1,0:T(4,128)} %bitcast.10, f32[1,4]{1,0:T(1,128)} %bitcast.14, ...), custom_call_target="tpu_custom_call" | custom-call | tf_op jit(solution)/shard_map/layer/pallas_call | solution.py:806
  164.0 1.7 %copy.22 = bf16[64,2048]{1,0:T(8,128)(2,1)} copy(bf16[64,2048]{1,0:T(8,128)(2,1)} %layer.1) | data formatting | bytes 524288

commit v6 on v5

--- a/solution.py
+++ b/solution.py
@@ -286,22 +286,66 @@
 
 def announce(nz, nx):
     z, c, x = lax.axis_index("sp_0"), lax.axis_index("sp_1"), lax.axis_index("tp")
+    place, quad = lax.rem(z, QUAD), z // QUAD
     barrier = pltpu.get_barrier_semaphore()
-
-    def along_z(k, carry):
-        pl.semaphore_signal(barrier, inc=1, device_id={"sp_0": lax.rem(z + k, nz)})
+    beyond = z + 2 * c - 1
+    has_beyond = (beyond >= 0) & (beyond < nz)
+    before = (place == 0) & (quad > 0)
+    behind = (place == QUAD - 1) & (quad < nz // QUAD - 1)
+
+    def in_quad(k, carry):
+        to = quad * QUAD + lax.rem(place + k, QUAD)
+        pl.semaphore_signal(barrier, inc=1, device_id={"sp_0": to})
         return carry
 
     def along_x(k, carry):
         pl.semaphore_signal(barrier, inc=1, device_id={"tp": lax.rem(x + k, nx)})
         return carry
 
-    lax.fori_loop(1, nz, along_z, 0)
+    pl.semaphore_signal(barrier, inc=1, device_id={"sp_1": 1 - c})
+    lax.fori_loop(1, QUAD, in_quad, 0)
     lax.fori_loop(1, nx, along_x, 0)
-    pl.semaphore_signal(barrier, inc=1, device_id={"sp_1": 1 - c})
-    pl.semaphore_signal(
-        barrier, inc=1, device_id={"sp_0": lax.rem(z + nz - 1 + 2 * c, nz), "sp_1": 1 - c}
-    )
+
+    @pl.when(has_beyond)
+    def _():
+        pl.semaphore_signal(barrier, inc=1, device_id={"sp_0": beyond, "sp_1": 1 - c})
+
+    @pl.when(before)
+    def _():
+        pl.semaphore_signal(barrier, inc=1, device_id={"sp_0": z - 1})
+
+    @pl.when(behind)
+    def _():
+        pl.semaphore_signal(barrier, inc=1, device_id={"sp_0": z + 1})
+
+    return QUAD + nx - 1 + sum(flag.astype(jnp.int32) for flag in (has_beyond, before, behind))
+
+
+def pass_word(nz, token, ready):
+    z = lax.axis_index("sp_0")
+    place, quad = lax.rem(z, QUAD), z // QUAD
+    last = nz // QUAD - 1
+
+    @pl.when((place == 0) & (quad > 0))
+    def _():
+        pl.semaphore_wait(token, 1)
+
+    @pl.when((place == 0) & (quad < last))
+    def _():
+        pl.semaphore_signal(token, inc=1, device_id={"sp_0": z + QUAD - 1})
+
+    @pl.when((place == QUAD - 1) & (quad < last))
+    def _():
+        pl.semaphore_wait(token, 1)
+        pl.semaphore_signal(token, inc=1, device_id={"sp_0": z + 1})
+
+    @pl.when((place == 0) & (quad == last))
+    def _():
+        def tell(k, carry):
+            pl.semaphore_signal(ready, inc=1, device_id={"sp_0": lax.rem(z + k, nz)})
+            return carry
+
+        lax.fori_loop(1, nz, tell, 0)
 
 
 def silu(v):
@@ -389,6 +433,8 @@
     rows,
     blend,
     turned,
+    smooth,
+    fading,
     blend_sem,
     halo_s,
     halo_r,
@@ -400,6 +446,8 @@
     far_r,
     gated_s,
     gated_r,
+    token,
+    ready,
 ):
     z, c, x = lax.axis_index("sp_0"), lax.axis_index("sp_1"), lax.axis_index("tp")
     length, width_x = xs_ref.shape
@@ -412,7 +460,7 @@
     quads = nz // QUAD
     f32, bf16 = jnp.float32, jnp.bfloat16
     partner = {"sp_1": 1 - c}
-    announce(nz, nx)
+    greeted = announce(nz, nx)
     load = pltpu.make_async_copy(blend_hbm, blend, blend_sem)
     load.start()
 
@@ -478,8 +526,29 @@
         noted = jnp.where(lane == 2 * picks + k, shares[:, k : k + 1], noted)
     facts[c] = noted
 
-    pl.semaphore_wait(pltpu.get_barrier_semaphore(), nz + nx)
     rim = halo.shape[0]
+    start = 0
+    for ref in (xs_ref, keys_ref, queries_ref):
+        joined[rim:, start : start + ref.shape[1]] = ref[...].astype(f32)
+        start += ref.shape[1]
+    taps = jnp.concatenate([taps_x_ref[...], taps_k_ref[...], taps_q_ref[...]], axis=1)
+    kernel_len = taps.shape[0]
+
+    def convolve(begin, end):
+        start = rim - kernel_len + 1
+        total = taps[0:1, :] * joined[start + begin : start + end, :]
+        for tap in range(1, kernel_len):
+            total = total + taps[tap : tap + 1, :] * joined[start + tap + begin : start + tap + end, :]
+        return silu(total)
+
+    smooth[rim:, :] = convolve(rim, length)
+    modulation = silu(gate_ref[...].astype(f32))
+    for h in range(heads):
+        between = running[:, h : h + 1] - running_row[h : h + 1, :]
+        fading[h] = jnp.exp(jnp.where(causal, between, -1e30))
+
+    pl.semaphore_wait(pltpu.get_barrier_semaphore(), greeted)
+    pass_word(nz, token, ready)
     after = {"sp_0": lax.rem(z + c, nz), "sp_1": 1 - c}
     edges = []
     start = 0
@@ -495,30 +564,31 @@
             )
         )
         start += ref.shape[1]
-    for edge in edges:
-        edge.start()
+
+    @pl.when(z + c < nz)
+    def _():
+        for edge in edges:
+            edge.start()
+
     facts_copy = pltpu.make_async_remote_copy(
         facts.at[c], facts.at[c], pair_s.at[0], pair_r.at[0], device_id=partner
     )
     facts_copy.start()
 
-    start = 0
-    for ref in (xs_ref, keys_ref, queries_ref):
-        joined[rim:, start : start + ref.shape[1]] = ref[...].astype(f32)
-        start += ref.shape[1]
-    for edge in edges:
-        edge.wait_recv()
-    joined[:rim, :] = jnp.where(z + c > 0, halo[...].astype(f32), 0.0)
-    taps = jnp.concatenate([taps_x_ref[...], taps_k_ref[...], taps_q_ref[...]], axis=1)
-    kernel_len = taps.shape[0]
-    convolved = taps[0:1, :] * joined[rim - kernel_len + 1 : rim - kernel_len + 1 + length, :]
-    for tap in range(1, kernel_len):
-        first = rim - kernel_len + 1 + tap
-        convolved = convolved + taps[tap : tap + 1, :] * joined[first : first + length, :]
-    convolved = silu(convolved)
-    inputs_x = convolved[:, :width_x]
-    keys_b = convolved[:, width_x : width_x + state_width].astype(bf16)
-    queries_c = convolved[:, width_x + state_width :].astype(bf16)
+    @pl.when(z + c > 0)
+    def _():
+        for edge in edges:
+            edge.wait_recv()
+        joined[:rim, :] = halo[...].astype(f32)
+
+    @pl.when(z + c == 0)
+    def _():
+        joined[:rim, :] = jnp.zeros_like(joined[:rim, :])
+
+    smooth[:rim, :] = convolve(0, rim)
+    inputs_x = smooth[:, :width_x]
+    keys_b = smooth[:, width_x : width_x + state_width].astype(bf16)
+    queries_c = smooth[:, width_x + state_width :].astype(bf16)
 
     scaled = [
         inputs_x[:, h * head_dim : (h + 1) * head_dim] * stride[:, h : h + 1] for h in range(heads)
@@ -541,11 +611,9 @@
     )
     inside = []
     for h in range(heads):
-        between = running[:, h : h + 1] - running_row[h : h + 1, :]
-        decays = jnp.exp(jnp.where(causal, between, -1e30))
         inside.append(
             jnp.dot(
-                (scores * decays).astype(bf16), scaled[h].astype(bf16), preferred_element_type=f32
+                (scores * fading[h]).astype(bf16), scaled[h].astype(bf16), preferred_element_type=f32
             )
         )
 
@@ -590,6 +658,11 @@
         whole = followed(whole, unpacked(quad_in[k], half_heads))
     far_out[...] = packed(*whole)
 
+    @pl.when((place > 0) | (quad < quads - 1))
+    def _():
+        pl.semaphore_wait(ready, 1)
+
+
     def far_send(k):
         return pltpu.make_async_remote_copy(
             far_out,
@@ -628,7 +701,6 @@
     )
     half_copy.start()
     kept = jnp.where(c == 0, incoming_low, incoming_high).astype(bf16)
-    modulation = silu(gate_ref[...].astype(f32))
     half_copy.wait_recv()
     sent_in = half_in[...]
     entering = jnp.concatenate(
@@ -714,8 +786,12 @@
         .reshape(outgoing_ref.shape)
     )
 
-    for edge in edges:
-        edge.wait_send()
+
+    @pl.when(z + c < nz)
+    def _():
+        for edge in edges:
+            edge.wait_send()
+
     facts_copy.wait_send()
     pair_copy.wait_send()
     half_copy.wait_send()
@@ -733,7 +809,7 @@
 
 
 FRONT_INPUTS = 17
-FRONT_SCRATCH = 27
+FRONT_SCRATCH = 31
 
 
 def layer_kernel(nz, nx, capacity, *refs):
@@ -781,6 +857,8 @@
         pltpu.VMEM((2, count, width), bf16),
         pltpu.VMEM(blend.shape, bf16),
         pltpu.VMEM((xs.shape[0], 128), f32),
+        pltpu.VMEM((xs.shape[0], total), f32),
+        pltpu.VMEM((raw.shape[0], xs.shape[0], xs.shape[0]), f32),
         pltpu.SemaphoreType.DMA,
         sems(3),
         sems(3),
@@ -792,6 +870,8 @@
         sems(nz // QUAD),
         sems(nx),
         sems(nx),
+        pltpu.SemaphoreType.REGULAR,
+        pltpu.SemaphoreType.REGULAR,
     ]
     experts_scratch = (
         [wide, wide, slots, slots, slots, slots, slots]

time: 166 us -> 163 us (0.982)
  Pallas kernels: 164 us -> 161 us
    pallas_call x1, Pallas kernels: 164 us -> 161 us  [layer(): pl.pallas_call(functools.partial(layer_kernel, nz, nx, capacity), out_sha...]
where the time goes in v6:
time: 163 us
  Pallas kernels  161 us (99%)
  local copies, waits for them, and re-layouts  1.67 us (1%)
    pallas_call x1, Pallas kernels, layer(): pl.pallas_call(functools.partial(layer_kernel, nz, nx, capacity), out_sha...  161 us

profile of v6, /device:TPU:33, one launch (start us, length us, event | category | flops | bytes accessed | tf_op | source)
XLA Modules:
  0.0 162.9 jit_solution(12630006205644794881)
XLA Ops:
  0.0 161.3 %layer.1 = bf16[64,2048]{1,0:T(8,128)(2,1)} custom-call(bf16[256,256]{1,0:T(8,128)(2,1)} %refs_0_.1, bf16[256,256]{1,0:T(8,128)(2,1)} %refs_1_.1, bf16[256,128]{1,0:T(8,128)(2,1)} %refs_2_.1, bf16[256,128]{1,0:T(8,128)(2,1)} %refs_3_.1, f32[4,256]{1,0:T(4,128)} %bitcast.9, f32[4,256]{1,0:T(4,128)} %bitcast.10, f32[1,4]{1,0:T(1,128)} %bitcast.14, ...), custom_call_target="tpu_custom_call" | custom-call | tf_op jit(solution)/shard_map/layer/pallas_call | solution.py:886
  161.3 1.7 %copy.22 = bf16[64,2048]{1,0:T(8,128)(2,1)} copy(bf16[64,2048]{1,0:T(8,128)(2,1)} %layer.1) | data formatting | bytes 524288

commit v7 on v6

--- a/solution.py
+++ b/solution.py
@@ -447,6 +447,7 @@
     gated_s,
     gated_r,
     token,
+    following,
     ready,
 ):
     z, c, x = lax.axis_index("sp_0"), lax.axis_index("sp_1"), lax.axis_index("tp")
@@ -548,7 +549,11 @@
         fading[h] = jnp.exp(jnp.where(causal, between, -1e30))
 
     pl.semaphore_wait(pltpu.get_barrier_semaphore(), greeted)
-    pass_word(nz, token, ready)
+
+    @pl.when((place == 0) & (quad > 0))
+    def _():
+        pl.semaphore_signal(following, inc=1, device_id={"sp_0": z - 1})
+
     after = {"sp_0": lax.rem(z + c, nz), "sp_1": 1 - c}
     edges = []
     start = 0
@@ -647,53 +652,55 @@
         )
 
     for k in range(1, QUAD):
-        quad_send(k).start()
-    quad_in[place] = quad_out[...]
+
+        @pl.when(place + k < QUAD)
+        def _(k=k):
+            quad_send(k).start()
+
+    pass_word(nz, token, ready)
     for k in range(1, QUAD):
-        quad_arrival(k).wait_recv()
+
+        @pl.when(place >= k)
+        def _(k=k):
+            quad_arrival(k).wait_recv()
+
+        @pl.when(place < k)
+        def _(k=k):
+            quad_in[k - 1] = jnp.zeros_like(quad_out)
+
     nothing = (jnp.zeros_like(chip[0]), [jnp.ones_like(d) for d in chip[1]])
-    whole, inner = nothing, nothing
-    for k in range(QUAD):
-        inner = chosen(place == k, whole, inner)
-        whole = followed(whole, unpacked(quad_in[k], half_heads))
-    far_out[...] = packed(*whole)
-
-    @pl.when((place > 0) | (quad < quads - 1))
-    def _():
-        pl.semaphore_wait(ready, 1)
-
+    inner = nothing
+    for k in range(QUAD - 1):
+        inner = chosen(k < place, followed(inner, unpacked(quad_in[k], half_heads)), inner)
 
     def far_send(k):
         return pltpu.make_async_remote_copy(
             far_out,
-            far_in.at[k],
+            far_in,
             far_s.at[k],
-            far_r.at[k],
-            device_id={"sp_0": lax.rem(z + k * QUAD, nz)},
+            far_r,
+            device_id={"sp_0": lax.rem(z + 1 + k, nz)},
         )
 
-    for k in range(1, quads):
-
-        @pl.when(quad + k < quads)
-        def _(k=k):
+    @pl.when(quad > 0)
+    def _():
+        far_send(0).wait_recv()
+
+    @pl.when(quad == 0)
+    def _():
+        far_in[...] = jnp.zeros_like(far_in)
+
+    incoming = followed((far_in[...].astype(f32), nothing[1]), inner)
+    incoming_low = incoming[0]
+    leads_on = (place == QUAD - 1) & (quad < quads - 1)
+
+    @pl.when(leads_on)
+    def _():
+        far_out[...] = followed(incoming, chip)[0].astype(bf16)
+        pl.semaphore_wait(following, 1)
+        for k in range(QUAD):
             far_send(k).start()
 
-    far_in[0] = jnp.zeros_like(far_out)
-    for k in range(1, quads):
-
-        @pl.when(quad >= k)
-        def _(k=k):
-            far_send(k).wait_recv()
-
-        @pl.when(quad < k)
-        def _(k=k):
-            far_in[k] = jnp.zeros_like(far_out)
-
-    incoming = nothing
-    for k in reversed(range(1, quads)):
-        incoming = followed(incoming, unpacked(far_in[k], half_heads))
-    incoming = followed(incoming, inner)
-    incoming_low = incoming[0]
     incoming_high = followed(incoming, lower)[0]
     half_out[...] = jnp.where(c == 0, incoming_high, incoming_low).astype(bf16)
     half_copy = pltpu.make_async_remote_copy(
@@ -797,19 +804,26 @@
     half_copy.wait_send()
     rows_copy.wait_send()
     for k in range(1, QUAD):
-        quad_send(k).wait_send()
-    for k in range(1, quads):
-
-        @pl.when(quad + k < quads)
+
+        @pl.when(place + k < QUAD)
         def _(k=k):
+            quad_send(k).wait_send()
+
+    @pl.when(leads_on)
+    def _():
+        for k in range(QUAD):
             far_send(k).wait_send()
 
     for k in range(1, nx):
         gated_send(k).wait_send()
 
+    @pl.when((place > 0) | (quad < quads - 1))
+    def _():
+        pl.semaphore_wait(ready, 1)
+
 
 FRONT_INPUTS = 17
-FRONT_SCRATCH = 31
+FRONT_SCRATCH = 32
 
 
 def layer_kernel(nz, nx, capacity, *refs):
@@ -847,8 +861,8 @@
         pltpu.VMEM((channels + TAIL, states), bf16),
         pltpu.VMEM((half + TAIL, states), bf16),
         pltpu.VMEM((QUAD, half + TAIL, states), bf16),
-        pltpu.VMEM((half + TAIL, states), bf16),
-        pltpu.VMEM((nz // QUAD, half + TAIL, states), bf16),
+        pltpu.VMEM((half, states), bf16),
+        pltpu.VMEM((half, states), bf16),
         pltpu.VMEM((half, states), bf16),
         pltpu.VMEM((half, states), bf16),
         pltpu.VMEM((nx, count, channels), bf16),
@@ -866,10 +880,11 @@
         sems(4),
         sems(QUAD),
         sems(QUAD),
-        sems(nz // QUAD),
-        sems(nz // QUAD),
+        sems(QUAD),
+        pltpu.SemaphoreType.DMA,
         sems(nx),
         sems(nx),
+        pltpu.SemaphoreType.REGULAR,
         pltpu.SemaphoreType.REGULAR,
         pltpu.SemaphoreType.REGULAR,
     ]

time: 163 us -> 162 us (level)
  no operation moved by 1% of the time
where the time goes in v7:
time: 162 us
  Pallas kernels  161 us (99%)
  local copies, waits for them, and re-layouts  1.67 us (1%)
    pallas_call x1, Pallas kernels, layer(): pl.pallas_call(functools.partial(layer_kernel, nz, nx, capacity), out_sha...  161 us

profile of v7, /device:TPU:33, one launch (start us, length us, event | category | flops | bytes accessed | tf_op | source)
XLA Modules:
  0.0 162.2 jit_solution(12694785475329831569)
XLA Ops:
  0.0 160.5 %layer.1 = bf16[64,2048]{1,0:T(8,128)(2,1)} custom-call(bf16[256,256]{1,0:T(8,128)(2,1)} %refs_0_.1, bf16[256,256]{1,0:T(8,128)(2,1)} %refs_1_.1, bf16[256,128]{1,0:T(8,128)(2,1)} %refs_2_.1, bf16[256,128]{1,0:T(8,128)(2,1)} %refs_3_.1, f32[4,256]{1,0:T(4,128)} %bitcast.9, f32[4,256]{1,0:T(4,128)} %bitcast.10, f32[1,4]{1,0:T(1,128)} %bitcast.14, ...), custom_call_target="tpu_custom_call" | custom-call | tf_op jit(solution)/shard_map/layer/pallas_call | solution.py:901
  160.6 1.7 %copy.22 = bf16[64,2048]{1,0:T(8,128)(2,1)} copy(bf16[64,2048]{1,0:T(8,128)(2,1)} %layer.1) | data formatting | bytes 524288

commit v8 on v7

--- a/solution.py
+++ b/solution.py
@@ -210,6 +210,11 @@
             for load in loads:
                 load.wait()
 
+        @pl.when(p > 1)
+        def _():
+            second(i - 4)
+            second(i - 3)
+
         @pl.when((p > 0) & (p <= pairs))
         def _():
             complete(i - 2)
@@ -218,25 +223,20 @@
             first(i - 2)
             first(i - 1)
 
-        @pl.when((p > 1) & (p <= pairs + 1))
+        @pl.when(p > 1)
         def _():
-            second(i - 4)
-            second(i - 3)
-
-        @pl.when(p > 2)
-        def _():
-            third(i - 6)
-            third(i - 5)
-
-            @pl.when(p > 3)
+            third(i - 4)
+            third(i - 3)
+
+            @pl.when(p > 2)
             def _():
-                send_back(i - 6).start()
-
-            send_back(i - 5).start()
+                send_back(i - 4).start()
+
+            send_back(i - 3).start()
 
         return carry
 
-    lax.fori_loop(0, pairs + 3, turn, 0)
+    lax.fori_loop(0, pairs + 2, turn, 0)
     own_back = pltpu.make_async_copy(total.at[0], answers.at[:, z], here.at[1])
     own_back.start()
     own_back.wait()

time: 162 us -> 158 us (0.975)
  Pallas kernels: 161 us -> 156 us
    pallas_call x1, Pallas kernels: 161 us -> 156 us  [layer(): pl.pallas_call(functools.partial(layer_kernel, nz, nx, capacity), out_sha...]
where the time goes in v8:
time: 158 us; the launch traced here: 157 us
  Pallas kernels  156 us (99%)
  local copies, waits for them, and re-layouts  1.67 us (1%)
    pallas_call x1, Pallas kernels, layer(): pl.pallas_call(functools.partial(layer_kernel, nz, nx, capacity), out_sha...  156 us

profile of v8, /device:TPU:33, one launch (start us, length us, event | category | flops | bytes accessed | tf_op | source)
XLA Modules:
  0.0 157.3 jit_solution(6730163548679138522)
XLA Ops:
  0.0 155.7 %layer.1 = bf16[64,2048]{1,0:T(8,128)(2,1)} custom-call(bf16[256,256]{1,0:T(8,128)(2,1)} %refs_0_.1, bf16[256,256]{1,0:T(8,128)(2,1)} %refs_1_.1, bf16[256,128]{1,0:T(8,128)(2,1)} %refs_2_.1, bf16[256,128]{1,0:T(8,128)(2,1)} %refs_3_.1, f32[4,256]{1,0:T(4,128)} %bitcast.9, f32[4,256]{1,0:T(4,128)} %bitcast.10, f32[1,4]{1,0:T(1,128)} %bitcast.14, ...), custom_call_target="tpu_custom_call" | custom-call | tf_op jit(solution)/shard_map/layer/pallas_call | solution.py:901
  155.7 1.7 %copy.22 = bf16[64,2048]{1,0:T(8,128)(2,1)} copy(bf16[64,2048]{1,0:T(8,128)(2,1)} %layer.1) | data formatting | bytes 524288
